TPU v7x, 32 devices: a whole 2x2x4 slice. The times are simulated.
32 devices in a mesh: sp: 8 (over z, x), dp: 4 (over y, core).
Axes of the slice: x: 2, y: 2, z: 4, core: 2. Of those that a mesh axis runs over, the one named last changes fastest.
Arguments:
- layer_activity: bfloat16 [4, 1024, 2048], P('dp', 'sp'), may hold values from -6 to 6
- writer_matrix: bfloat16 [2048, 256], P('dp'), may hold values from -0.125 to 0.125
- reader_matrix: bfloat16 [2048, 256], P('dp'), may hold values from -0.125 to 0.125
- source_unfiltered: bfloat16 [4, 1024, 2048], P('dp', 'sp'), may hold values from -6 to 6
- switch_raw_signal: bfloat16 [4, 1024, 2048], P('dp', 'sp'), may hold values from -6 to 6
- saved_result: bfloat16 [4, 1024, 2048], P('dp', 'sp'), may hold values from -6 to 6
- final_adjoint: bfloat16 [4, 1024, 2048], P('dp', 'sp'), may hold values from -6 to 6
- delta_raw: bfloat16 [4, 1024, 32], P('dp', 'sp'), may hold values from -4 to 4
- extra_logdrop: float32 [4, 1024, 32], P('dp', None, 'sp'), may hold values from 0 to 2.1
- source_filter_coefs: float32 [5, 2048], P(None, 'sp'), may hold values from -2.5 to 2.5
- writer_filter_coefs: float32 [5, 256], replicated, may hold values from -2.5 to 2.5
- reader_filter_coefs: float32 [5, 256], replicated, may hold values from -2.5 to 2.5
- delta_offset: float32 [32], P('sp'), may hold values from -7.5 to -6
- fading_exponents: float32 [32], P('sp'), may hold values from -6 to 3.4
- direct_factor: float32 [32], P('sp'), may hold values from 0.1 to 1.9
- rescale_factor: float32 [2048], replicated, may hold values from 0.1 to 1.9
Outputs:
- d_hidden: bfloat16 [4, 1024, 2048], P('dp', 'sp')
- d_x_raw: bfloat16 [4, 1024, 2048], P('dp', 'sp')
- d_gate: bfloat16 [4, 1024, 2048], P('dp', 'sp')
- d_dt_raw: bfloat16 [4, 1024, 32], P('dp', 'sp')
- d_w_b: float32 [2048, 256], P('dp')
- d_w_c: float32 [2048, 256], P('dp')
All inputs are finite; a program needn't handle non-finite values.
Results may differ from a plain program's by a relative error of at most 0.012.
Values may be sent and summed in bfloat16 or wider, within the bound.
A program may use at most 128 MiB of HBM per device.

v0:
```python
import functools

import jax
import jax.numpy as jnp
from jax import lax
from jax.experimental import pallas as pl
from jax.experimental.pallas import tpu as pltpu
from jax.sharding import PartitionSpec as P

HEADS = 32
HEAD_DIM = 64
STATE = 128
GROUPS = 2
NORM_GROUPS = 8
CONV_K = 5
BLOCK = 128
INNER = 2048
LANES = 128
DT_ROWS = 16
HALO = 8
EPSILON = 1e-06
LOG2E = 1.4426950408889634
highest = lax.Precision.HIGHEST
f32 = jnp.float32
bf16 = jnp.bfloat16


def sigmoid(v):
    return 1.0 / (1.0 + jnp.exp(-v))


def softplus(v):
    e = jnp.exp(-jnp.abs(v))
    z = e / (2.0 + e)
    z2 = z * z
    series = jnp.full_like(z, 1.0 / 17.0)
    for odd in (15, 13, 11, 9, 7, 5, 3, 1):
        series = series * z2 + 1.0 / odd
    return jnp.maximum(v, 0.0) + 2.0 * z * series


def window_conv(padded, r0, taps, flip):
    rows = padded[pl.ds(r0, BLOCK + 2 * HALO), :]
    total = None
    for k in range(CONV_K):
        shift = HALO - CONV_K // 2 + k
        tap = taps[CONV_K - 1 - k if flip else k][None, :]
        term = tap * pltpu.roll(rows, rows.shape[0] - shift, axis=0)[:BLOCK]
        total = term if total is None else total + term
    return total


def mixer_kernel(
    heads,
    tile,
    x_ref,
    dt_ref,
    dy_ref,
    bc_ref,
    drop_ref,
    tapx_ref,
    tapbc_ref,
    par_ref,
    dx_ref,
    dbc_ref,
    ddt_ref,
    pad_x,
    pad_bc,
    u_ref,
    sux_ref,
    sbc_ref,
    dtc_ref,
    sig_ref,
    lcol,
    lrow,
    kt,
    rt,
    kn,
    rn,
    vt,
    dyt,
    dyh,
    dvt,
    dkt,
    dr,
    rowacc,
    rowdl,
    colsum,
):
    window = x_ref.shape[0]
    xw = u_ref.shape[1]
    chunks = window // BLOCK
    tapx = tapx_ref[...]
    tapbc = tapbc_ref[...]
    offset = par_ref[0:1, :]
    fade = par_ref[1:2, :]
    skip = tapx[CONV_K : CONV_K + 1]
    lane_head = lax.broadcasted_iota(jnp.int32, (BLOCK, xw), 1) // HEAD_DIM
    row_i = lax.broadcasted_iota(jnp.int32, (BLOCK, BLOCK), 0)
    col_i = lax.broadcasted_iota(jnp.int32, (BLOCK, BLOCK), 1)
    lower = (row_i >= col_i).astype(f32)
    upper = (row_i <= col_i).astype(f32)

    def spread(columns):
        out = jnp.zeros((BLOCK, xw), f32)
        for h in range(heads):
            out = jnp.where(lane_head == h, columns[:, h : h + 1], out)
        return out

    for padded in (pad_x, pad_bc):
        padded[0:HALO, :] = jnp.zeros((HALO, padded.shape[1]), f32)
        padded[HALO + window :, :] = jnp.zeros((HALO, padded.shape[1]), f32)

    @pl.loop(0, chunks)
    def _(c):
        r0 = pl.multiple_of(c * BLOCK, BLOCK)
        rows = pl.ds(r0, BLOCK)
        into = pl.ds(pl.multiple_of(r0 + HALO, HALO), BLOCK)
        pad_x[into, :] = x_ref[rows, :].astype(f32)
        pad_bc[into, :] = bc_ref[rows, :].astype(f32)

    def prepare(c, carry):
        r0 = pl.multiple_of(c * BLOCK, BLOCK)
        rows = pl.ds(r0, BLOCK)
        steps = dt_ref[c].astype(f32)
        steps = jnp.concatenate([steps, jnp.zeros((LANES - DT_ROWS, BLOCK), f32)]).T
        a = steps + offset
        dt = softplus(a)
        dtc_ref[rows, :] = dt
        sig_ref[rows, :] = sigmoid(a)
        rate = dt * fade + drop_ref[rows, :]
        level = jnp.dot(lower, rate, precision=highest, preferred_element_type=f32) + carry
        scaled = level * LOG2E
        lcol[rows, :] = scaled
        lrow[:, rows] = scaled.T[: lrow.shape[0]]
        pre = window_conv(pad_x, r0, tapx, False)
        sig = sigmoid(pre)
        u = pre * sig
        u_ref[rows, :] = u
        sux_ref[rows, :] = sig + u * (1.0 - sig)
        vt[:, rows] = (u * spread(dt)).T.astype(bf16)
        dy_t = dy_ref[rows, :].astype(f32).T
        dyt[:, rows] = dy_t.astype(bf16)
        for h in range(heads):
            dyh[h, rows, :] = dy_t[h * HEAD_DIM : (h + 1) * HEAD_DIM].T.astype(bf16)
        pre = window_conv(pad_bc, r0, tapbc, False)
        sig = sigmoid(pre)
        kr = pre * sig
        sbc_ref[rows, :] = sig + kr * (1.0 - sig)
        kn[rows, :] = kr[:, :STATE].astype(bf16)
        rn[rows, :] = kr[:, STATE:].astype(bf16)
        kt[:, rows] = kr[:, :STATE].T.astype(bf16)
        rt[:, rows] = kr[:, STATE:].T.astype(bf16)
        return level[BLOCK - 1 : BLOCK]

    lax.fori_loop(0, chunks, prepare, jnp.zeros((1, LANES), f32))

    dvt[...] = jnp.zeros_like(dvt)
    dkt[...] = jnp.zeros_like(dkt)
    colsum[...] = jnp.zeros_like(colsum)
    rowdl[...] = jnp.zeros_like(rowdl)
    ahead = lax.broadcasted_iota(jnp.int32, (tile, tile), 0) - lax.broadcasted_iota(
        jnp.int32, (tile, tile), 1
    )

    @pl.loop(0, window // tile)
    def _(ti):
        t0 = pl.multiple_of(ti * tile, tile)
        ts = pl.ds(t0, tile)
        rowacc[...] = jnp.zeros_like(rowacc)
        dr[ts, :] = jnp.zeros((tile, STATE), f32)
        reads = rn[ts, :]
        reads_t = rt[:, ts]

        @pl.loop(0, window // tile)
        def _(si):
            s0 = pl.multiple_of(si * tile, tile)
            ss = pl.ds(s0, tile)
            score = jnp.dot(reads, kt[:, ss], preferred_element_type=f32)
            order = jnp.clip(ahead + (t0 - s0), -1, 1).astype(f32)
            signed = score * order
            ge_sum = None
            for h in range(heads):
                hs = slice(h * HEAD_DIM, (h + 1) * HEAD_DIM)
                gap = lcol[ts, h : h + 1] - lrow[h : h + 1, ss]
                decay = jnp.exp2(-jnp.abs(gap))
                g = jnp.dot(dyh[h, ts, :], vt[hs, ss], preferred_element_type=f32)
                ge = g * decay
                ge_sum = ge if ge_sum is None else ge_sum + ge
                se = (score * decay).astype(bf16)
                dvt[hs, ss] += jnp.dot(dyt[hs, ts], se, preferred_element_type=f32)
                pair = signed * ge
                colsum[h : h + 1, ss] += jnp.sum(pair, axis=0, keepdims=True)
                part = pair[:, :LANES]
                for piece in range(1, tile // LANES):
                    part = part + pair[:, piece * LANES : (piece + 1) * LANES]
                rowacc[h] += part
            ge_b = ge_sum.astype(bf16)
            dr[ts, :] += jnp.dot(ge_b, kn[ss, :], preferred_element_type=f32)
            dkt[:, ss] += jnp.dot(reads_t, ge_b, preferred_element_type=f32)

        for h in range(heads):
            rowdl[ts, h : h + 1] = -jnp.sum(rowacc[h], axis=1, keepdims=True)

    def finish(i, carry):
        r0 = pl.multiple_of((chunks - 1 - i) * BLOCK, BLOCK)
        rows = pl.ds(r0, BLOCK)
        into = pl.ds(pl.multiple_of(r0 + HALO, HALO), BLOCK)
        dlevel = rowdl[rows, :] + colsum[:, rows].T
        drate = jnp.dot(upper, dlevel, precision=highest, preferred_element_type=f32) + carry
        dv = dvt[:, rows].T
        u = u_ref[rows, :]
        udv = u * dv
        lane = lax.broadcasted_iota(jnp.int32, (BLOCK, LANES), 1)
        ddt = drate * fade
        for h in range(heads):
            along = jnp.sum(jnp.where(lane_head == h, udv, 0.0), axis=1, keepdims=True)
            ddt = ddt + jnp.where(lane == h, along, 0.0)
        ddt_ref[chunks - 1 - i] = (ddt * sig_ref[rows, :]).T[:DT_ROWS].astype(bf16)
        du = dv * spread(dtc_ref[rows, :]) + skip * dy_ref[rows, :].astype(f32)
        pad_x[into, :] = du * sux_ref[rows, :]
        sbc = sbc_ref[rows, :]
        pad_bc[into, :STATE] = dkt[:, rows].T * sbc[:, :STATE]
        pad_bc[into, STATE:] = dr[rows, :] * sbc[:, STATE:]
        return carry + jnp.sum(dlevel, axis=0, keepdims=True)

    lax.fori_loop(0, chunks, finish, jnp.zeros((1, LANES), f32))

    @pl.loop(0, chunks)
    def _(c):
        r0 = pl.multiple_of(c * BLOCK, BLOCK)
        rows = pl.ds(r0, BLOCK)
        dx_ref[rows, :] = window_conv(pad_x, r0, tapx, True).astype(bf16)
        dbc_ref[rows, :] = window_conv(pad_bc, r0, tapbc, True).astype(bf16)


def mixer_backward(x, dt, dy, bc, drop, tapx, tapbc, par, heads):
    window = x.shape[0]
    xw = tapx.shape[1]
    tile = 2 * BLOCK if window % (2 * BLOCK) == 0 else BLOCK
    rows_h = -(-heads // 8) * 8
    scratch = [
        pltpu.VMEM((window + 2 * HALO, xw), f32),
        pltpu.VMEM((window + 2 * HALO, 2 * STATE), f32),
        pltpu.VMEM((window, xw), f32),
        pltpu.VMEM((window, xw), f32),
        pltpu.VMEM((window, 2 * STATE), f32),
        pltpu.VMEM((window, LANES), f32),
        pltpu.VMEM((window, LANES), f32),
        pltpu.VMEM((window, LANES), f32),
        pltpu.VMEM((rows_h, window), f32),
        pltpu.VMEM((STATE, window), bf16),
        pltpu.VMEM((STATE, window), bf16),
        pltpu.VMEM((window, STATE), bf16),
        pltpu.VMEM((window, STATE), bf16),
        pltpu.VMEM((xw, window), bf16),
        pltpu.VMEM((xw, window), bf16),
        pltpu.VMEM((heads, window, HEAD_DIM), bf16),
        pltpu.VMEM((xw, window), f32),
        pltpu.VMEM((STATE, window), f32),
        pltpu.VMEM((window, STATE), f32),
        pltpu.VMEM((heads, tile, LANES), f32),
        pltpu.VMEM((window, LANES), f32),
        pltpu.VMEM((LANES, window), f32),
    ]
    return pl.pallas_call(
        functools.partial(mixer_kernel, heads, tile),
        in_specs=[pl.BlockSpec(memory_space=pltpu.VMEM)] * 8,
        out_specs=[pl.BlockSpec(memory_space=pltpu.VMEM)] * 3,
        out_shape=[
            jax.ShapeDtypeStruct((window, xw), bf16),
            jax.ShapeDtypeStruct((window, 2 * STATE), bf16),
            jax.ShapeDtypeStruct(dt.shape, bf16),
        ],
        scratch_shapes=scratch,
        compiler_params=pltpu.CompilerParams(vmem_limit_bytes=62 * 1024 * 1024),
        name="mixer_backward",
    )(x, dt, dy, bc, drop, tapx, tapbc, par)


def pad_last(values, width):
    pads = [(0, 0)] * (values.ndim - 1) + [(0, width - values.shape[-1])]
    return jnp.pad(values, pads)


def by_owner(values, owners):
    tokens, width = values.shape
    return jnp.transpose(values.reshape(tokens, owners, width // owners), (1, 0, 2))


def greet(axes):
    barrier = pltpu.get_barrier_semaphore()
    count = 0
    for axis in axes:
        size = lax.axis_size(axis)
        me = lax.axis_index(axis)
        for o in range(1, size):
            pl.semaphore_signal(
                barrier,
                inc=1,
                device_id={axis: lax.rem(me + o, size)},
                device_id_type=pl.DeviceIdType.MESH,
            )
            count += 1
    pl.semaphore_wait(barrier, count)


def send_all(axis, source, target, sems, slot):
    size = lax.axis_size(axis)
    me = lax.axis_index(axis)
    copies = []
    for o in range(1, size):
        peer = lax.rem(me + o, size)
        copies.append(
            pltpu.make_async_remote_copy(
                src_ref=source(peer),
                dst_ref=target(me),
                send_sem=sems.at[slot, 0, o],
                recv_sem=sems.at[slot, 1, o],
                device_id={axis: peer},
                device_id_type=pl.DeviceIdType.MESH,
            )
        )
    for copy in copies:
        copy.start()
    return copies


def received(copies):
    for copy in copies:
        copy.wait_recv()


def lanes_of(index, width):
    return pl.ds(pl.multiple_of(index * width, LANES), width)


def front_kernel(
    heads,
    la_ref,
    w_ref,
    x_ref,
    dt_ref,
    values_ref,
    gates_ref,
    adjoint_ref,
    scale_ref,
    cols_ref,
    xall_ref,
    dtall_ref,
    dyall_ref,
    bcall_ref,
    dgate_ref,
    dysend,
    psend,
    pall,
    bcsend,
    sems,
):
    dp = lax.axis_size("dp")
    sp = lax.axis_size("sp")
    me_dp = lax.axis_index("dp")
    me_sp = lax.axis_index("sp")
    tokens, width_in = la_ref.shape
    cw = width_in // dp
    xc = heads * HEAD_DIM
    per_group = HEADS // GROUPS
    greet(("dp", "sp"))
    la_copies = send_all(
        "dp", lambda p: la_ref.at[:, lanes_of(p, cw)], lambda m: cols_ref.at[m], sems, 0
    )
    x_copies = send_all("sp", lambda p: x_ref.at[p], lambda m: xall_ref.at[m], sems, 1)
    dt_copies = send_all("sp", lambda p: dt_ref.at[p], lambda m: dtall_ref.at[m], sems, 2)
    cols_ref[me_dp] = la_ref[:, lanes_of(me_dp, cw)]
    xall_ref[me_sp] = x_ref[me_sp]
    dtall_ref[me_sp] = dt_ref[me_sp]

    inner = values_ref.shape[1]
    width = inner // NORM_GROUPS
    for group in range(NORM_GROUPS):
        span = slice(group * width, (group + 1) * width)
        values = values_ref[:, span].astype(f32)
        gates = gates_ref[:, span].astype(f32)
        sig = sigmoid(gates)
        act = gates * sig
        g = values * act
        dn = adjoint_ref[:, span].astype(f32) * scale_ref[:, span]
        inv = lax.rsqrt(jnp.sum(g * g, axis=1, keepdims=True) * (1.0 / width) + EPSILON)
        along = jnp.sum(dn * g, axis=1, keepdims=True) * (1.0 / width)
        dg = inv * dn - g * (inv * inv * inv * along)
        dgate_ref[:, span] = (dg * values * (sig + act * (1.0 - sig))).astype(bf16)
        dy = (dg * act).astype(bf16)
        step = min(width, xc)
        for part in range(width // step):
            at = group * width + part * step
            owner, first = at // xc, at % xc
            dysend[owner, :, first : first + step] = dy[:, part * step : (part + 1) * step]
            if xc < dysend.shape[2]:
                dysend[owner, :, xc:] = jnp.zeros((tokens, dysend.shape[2] - xc), bf16)
    dy_copies = send_all("sp", lambda p: dysend.at[p], lambda m: dyall_ref.at[m], sems, 3)
    dyall_ref[me_sp] = dysend[me_sp]

    received(la_copies)
    for i in range(dp):
        psend[i] = jnp.dot(cols_ref[i], w_ref[...], preferred_element_type=f32).astype(bf16)
    p_copies = send_all("dp", lambda p: psend.at[p], lambda m: pall.at[m], sems, 4)
    total = psend[me_dp].astype(f32)
    pall[me_dp] = jnp.zeros(pall.shape[1:], bf16)
    received(p_copies)
    for i in range(dp):
        total = total + pall[i].astype(f32)
    total = total.astype(bf16)
    for group in range(GROUPS):
        at = group * STATE
        bcsend[group, :, :STATE] = total[:, at : at + STATE]
        at = (GROUPS + group) * STATE
        bcsend[group, :, STATE:] = total[:, at : at + STATE]
    bc_copies = send_all(
        "sp",
        lambda p: bcsend.at[(p * heads) // per_group],
        lambda m: bcall_ref.at[m],
        sems,
        5,
    )
    bcall_ref[me_sp] = bcsend[(me_sp * heads) // per_group]
    for copies in (x_copies, dt_copies, dy_copies, bc_copies):
        received(copies)
    for copies in (la_copies, x_copies, dt_copies, dy_copies, p_copies, bc_copies):
        for copy in copies:
            copy.wait_send()


def back_kernel(
    heads,
    dx_ref,
    dbc_ref,
    ddt_ref,
    cols_ref,
    w_ref,
    dxout_ref,
    ddtout_ref,
    dh_ref,
    dwb_ref,
    dwc_ref,
    dbcall,
    gall,
    gsend,
    wsend,
    wall,
    hsend,
    ssend,
    tall,
    sems,
):
    dp = lax.axis_size("dp")
    sp = lax.axis_size("sp")
    me_dp = lax.axis_index("dp")
    me_sp = lax.axis_index("sp")
    tokens = dx_ref.shape[1]
    cw = w_ref.shape[0]
    xc = heads * HEAD_DIM
    latent = GROUPS * STATE
    direct = xc % LANES == 0
    rows = cw // sp
    greet(("dp", "sp"))
    dbc_copies = send_all("sp", lambda p: dbc_ref.at[p], lambda m: dbcall.at[m], sems, 0)
    if direct:
        dx_to = lambda m: dxout_ref.at[:, lanes_of(m, xc)]
    else:
        dx_to = lambda m: dxout_ref.at[m]
    dx_copies = send_all("sp", lambda p: dx_ref.at[p], dx_to, sems, 1)
    ddt_copies = send_all("sp", lambda p: ddt_ref.at[p], lambda m: ddtout_ref.at[m], sems, 2)
    dbcall[me_sp] = dbc_ref[me_sp]
    ddtout_ref[me_sp] = ddt_ref[me_sp]
    if direct:
        dxout_ref[:, lanes_of(me_sp, xc)] = dx_ref[me_sp]
    else:
        dxout_ref[me_sp] = dx_ref[me_sp]
    received(dbc_copies)
    members = sp // GROUPS
    for group in range(GROUPS):
        total = dbcall[group * members].astype(f32)
        for member in range(1, members):
            total = total + dbcall[group * members + member].astype(f32)
        total = total.astype(bf16)
        at = group * STATE
        gsend[:, at : at + STATE] = total[:, :STATE]
        at = (GROUPS + group) * STATE
        gsend[:, at : at + STATE] = total[:, STATE:]
    g_copies = send_all("dp", lambda p: gsend, lambda m: gall.at[m], sems, 3)
    gall[me_dp] = gsend[...]
    received(g_copies)
    total = None
    for i in range(dp):
        term = lax.dot_general(
            cols_ref[i], gall[i], (((0,), (0,)), ((), ())), preferred_element_type=f32
        )
        total = term if total is None else total + term
    wsend[...] = total.astype(bf16).reshape(sp, rows, 2 * latent)
    w_copies = send_all("sp", lambda p: wsend.at[p], lambda m: wall.at[m], sems, 4)
    wall[me_sp] = wsend[me_sp]
    for i in range(dp):
        hsend[i] = lax.dot_general(
            gall[i], w_ref[...], (((1,), (1,)), ((), ())), preferred_element_type=f32
        ).astype(bf16)
    h_copies = send_all(
        "dp", lambda p: hsend.at[p], lambda m: dh_ref.at[:, lanes_of(m, cw)], sems, 5
    )
    dh_ref[:, lanes_of(me_dp, cw)] = hsend[me_dp]
    received(w_copies)
    share = wall[0].astype(f32)
    for j in range(1, sp):
        share = share + wall[j].astype(f32)
    ssend[...] = share.astype(bf16)
    s_copies = send_all("sp", lambda p: ssend, lambda m: tall.at[m], sems, 6)
    tall[me_sp] = ssend[...]
    received(s_copies)
    for j in range(sp):
        dwb_ref[j] = tall[j, :, :latent].astype(f32)
        dwc_ref[j] = tall[j, :, latent:].astype(f32)
    for copies in (dx_copies, ddt_copies, h_copies):
        received(copies)
    for copies in (
        dbc_copies,
        dx_copies,
        ddt_copies,
        g_copies,
        w_copies,
        h_copies,
        s_copies,
    ):
        for copy in copies:
            copy.wait_send()


def comm_call(kernel, args, shapes, scratch, slots, peers, number, name):
    vmem = pl.BlockSpec(memory_space=pltpu.VMEM)
    return pl.pallas_call(
        kernel,
        in_specs=[vmem] * len(args),
        out_specs=[vmem] * len(shapes),
        out_shape=[jax.ShapeDtypeStruct(shape, kind) for shape, kind in shapes],
        scratch_shapes=[pltpu.VMEM(shape, bf16) for shape in scratch]
        + [pltpu.SemaphoreType.DMA((slots, 2, peers))],
        compiler_params=pltpu.CompilerParams(
            collective_id=number, has_side_effects=True, vmem_limit_bytes=60 * 1024 * 1024
        ),
        name=name,
    )(*args)


def local(
    layer_activity,
    writer_matrix,
    reader_matrix,
    source_unfiltered,
    switch_raw_signal,
    saved_result,
    final_adjoint,
    delta_raw,
    extra_logdrop,
    source_filter_coefs,
    writer_filter_coefs,
    reader_filter_coefs,
    delta_offset,
    fading_exponents,
    direct_factor,
    rescale_factor,
):
    tokens = layer_activity.shape[1]
    width_in = layer_activity.shape[2]
    latent = GROUPS * STATE
    dp = lax.axis_size("dp")
    sp = lax.axis_size("sp")
    heads = delta_offset.shape[0]
    per_group = HEADS // GROUPS
    xc = heads * HEAD_DIM
    xw = -(-xc // LANES) * LANES
    window = tokens * sp
    cw = width_in // dp
    peers = max(sp, dp)

    weights = jnp.concatenate([writer_matrix, reader_matrix], axis=1)
    x_by = pad_last(by_owner(source_unfiltered.reshape(tokens, INNER), sp), xw)
    dt_by = delta_raw.reshape(tokens, HEADS).T.reshape(sp, heads, tokens)
    dt_by = jnp.pad(dt_by, ((0, 0), (0, DT_ROWS - heads), (0, 0)))
    cols, x_all, dt_all, dy_all, bc_all, d_gate = comm_call(
        functools.partial(front_kernel, heads),
        (
            layer_activity.reshape(tokens, width_in),
            weights,
            x_by,
            dt_by,
            saved_result.reshape(tokens, INNER),
            switch_raw_signal.reshape(tokens, INNER),
            final_adjoint.reshape(tokens, INNER),
            rescale_factor.reshape(1, INNER),
        ),
        (
            ((dp, tokens, cw), bf16),
            ((sp, tokens, xw), bf16),
            ((sp, DT_ROWS, tokens), bf16),
            ((sp, tokens, xw), bf16),
            ((sp, tokens, 2 * STATE), bf16),
            ((tokens, INNER), bf16),
        ),
        (
            (sp, tokens, xw),
            (dp, tokens, 2 * latent),
            (dp, tokens, 2 * latent),
            (GROUPS, tokens, 2 * STATE),
        ),
        6,
        peers,
        0,
        "front",
    )

    group = lax.axis_index("sp") * heads // per_group
    tapbc = jnp.concatenate(
        [
            lax.dynamic_slice_in_dim(writer_filter_coefs, group * STATE, STATE, axis=1),
            lax.dynamic_slice_in_dim(reader_filter_coefs, group * STATE, STATE, axis=1),
        ],
        axis=1,
    )
    par = pad_last(jnp.stack([delta_offset, jnp.exp(fading_exponents)]), LANES)
    dx, dbc, ddt = mixer_backward(
        x_all.reshape(window, xw),
        dt_all,
        dy_all.reshape(window, xw),
        bc_all.reshape(window, 2 * STATE),
        pad_last(extra_logdrop.reshape(window, heads), LANES),
        pad_last(
            jnp.concatenate([source_filter_coefs, jnp.repeat(direct_factor, HEAD_DIM)[None]]), xw
        ),
        tapbc,
        par,
        heads,
    )
    rows = cw // sp
    back_x, back_dt, d_hidden, d_w_b, d_w_c = comm_call(
        functools.partial(back_kernel, heads),
        (
            dx.reshape(sp, tokens, xw),
            dbc.reshape(sp, tokens, 2 * STATE),
            ddt,
            cols,
            weights,
        ),
        (
            ((tokens, INNER) if xc % LANES == 0 else (sp, tokens, xw), bf16),
            ((sp, DT_ROWS, tokens), bf16),
            ((tokens, width_in), bf16),
            ((sp, rows, latent), f32),
            ((sp, rows, latent), f32),
        ),
        (
            (sp, tokens, 2 * STATE),
            (dp, tokens, 2 * latent),
            (tokens, 2 * latent),
            (sp, rows, 2 * latent),
            (sp, rows, 2 * latent),
            (dp, tokens, cw),
            (rows, 2 * latent),
            (sp, rows, 2 * latent),
        ),
        7,
        peers,
        1,
        "back",
    )
    if xc % LANES:
        back_x = jnp.transpose(back_x[:, :, :xc], (1, 0, 2))
    back_dt = back_dt[:, :heads].reshape(HEADS, tokens).T
    return (
        d_hidden.reshape(1, tokens, width_in),
        back_x.reshape(1, tokens, INNER),
        d_gate.reshape(1, tokens, INNER),
        back_dt.reshape(1, tokens, HEADS),
        d_w_b.reshape(cw, latent),
        d_w_c.reshape(cw, latent),
    )


def solution(mesh):
    in_specs = (
        P("dp", "sp", None),
        P("dp", None),
        P("dp", None),
        P("dp", "sp", None),
        P("dp", "sp", None),
        P("dp", "sp", None),
        P("dp", "sp", None),
        P("dp", "sp", None),
        P("dp", None, "sp"),
        P(None, "sp"),
        P(),
        P(),
        P("sp"),
        P("sp"),
        P("sp"),
        P(),
    )
    out_specs = (
        P("dp", "sp", None),
        P("dp", "sp", None),
        P("dp", "sp", None),
        P("dp", "sp", None),
        P("dp", None),
        P("dp", None),
    )
    return jax.shard_map(local, mesh=mesh, in_specs=in_specs, out_specs=out_specs, check_vma=False)
```

profile of v0, /device:TPU:0, one launch (start us, length us, event | category | flops | bytes accessed | tf_op | source)
XLA Modules:
  0.0 140.2 jit_solution(3912675385528368304)
XLA Ops:
  0.7 0.0 copy-start.14
  0.7 0.0 copy-start.13
  0.7 0.0 copy-start.8
  0.7 0.6 copy-done.14
  1.3 0.0 copy-done.13
  1.3 0.0 copy-start.12
  1.3 0.5 select_maximum_fusion.par_ref
  1.9 0.1 copy-done.12
  2.0 0.1 broadcast_in_dim.3
  2.1 0.1 broadcast_in_dim_reshape.3
  2.1 0.0 copy-done.8
  2.1 0.0 copy-start.10
  2.1 0.0 copy-start.11
  2.1 0.6 pad_maximum_fusion.tapx_ref
  2.7 0.1 copy-done.10
  2.8 0.0 copy-done.11
  2.9 0.0 copy-start.9
  2.9 0.6 pad_maximum_fusion.1.tapbc_ref
  3.5 0.1 copy-done.9
  3.6 0.0 copy-start.6
  3.6 0.6 pad.12.dt_ref
  4.2 0.0 copy-start.1
  4.2 1.0 constant_dynamic-update-slice_fusion.1
  5.2 0.0 copy-done.6
  5.3 0.1 copy-done.1
  5.3 0.0 copy-start
  5.3 0.3 copy.23
  5.6 0.5 copy-done
  6.1 0.0 copy-start.7
  6.1 1.0 copy.24
  7.1 0.0 copy-done.7
  7.1 0.2 copy.25
  7.4 0.8 pad.13.drop_ref
  8.2 42.7 %front.1 = (bf16[4,128,512]{2,1,0:T(8,128)(2,1)}, bf16[8,128,256]{2,1,0:T(8,128)(2,1)}, bf16[8,16,128]{2,1,0:T(8,128)(2,1)}, bf16[8,128,256]{2,1,0:T(8,128)(2,1)...) custom-call(bf16[128,2048]{1,0:T(8,128)(2,1)} %bitcast.34, bf16[512,512]{1,0:T(8,128)(2,1)} %copy-done, ...), custom_call_target="tpu_custom_call" | custom-call | tf_op jit(solution)/shard_map/front/pallas_call | solution.py:538
  50.9 26.3 %mixer_backward.1 = (bf16[1024,256]{1,0:T(8,128)(2,1)}, bf16[1024,256]{1,0:T(8,128)(2,1)}, bf16[8,16,128]{2,1,0:T(8,128)(2,1)}) custom-call(bf16[1024,256]{1,0:T(8,128)(2,1)} %bitcast.45, bf16[8,16,128]{2,1,0:T(8,128)(2,1)} %get-tuple-element.21.dt_ref, bf16[1024,256]{1,0:T(8,128)(2,1)} %bitcast.46, bf16[1024,256]{1,0:T(8,128)(2,1)} %bitcast.47, ...), custom_call_target="tpu_custom_call" | custom-call | tf_op jit(solution)/shard_map/mixer_backward/pallas_call | solution.py:266
  77.2 55.2 %back.1 = (bf16[128,2048]{1,0:T(8,128)(2,1)}, bf16[8,16,128]{2,1,0:T(8,128)(2,1)}, bf16[128,2048]{1,0:T(8,128)(2,1)}, f32[8,64,256]{2,1,0:T(8,128)}, f32[8,64,256]{2,1,0:T(8,128)}) custom-call(bf16[8,128,256]{2,1,0:T(8,128)(2,1)} %bitcast.43, bf16[8,128,256]{2,1,0:T(8,128)(2,1)} %bitcast.44, bf16[8,16,128]{2,1,0:T(8,128)(2,1)} %get-tuple-element.26.ddt_ref, ...), custom_call_target="tpu_custom_call" | custom-call | tf_op jit(solution)/shard_map/back/pallas_call | solution.py:538
  132.4 1.3 slice.3
  133.7 0.0 copy-start.5
  133.7 1.9 %copy.32 = bf16[1,128,2048]{2,1,0:T(8,128)(2,1)} copy(bf16[1,128,2048]{2,1,0:T(8,128)(2,1)} %bitcast.42) | data formatting | bytes 1048576
  135.7 0.0 copy-done.5
  135.7 0.0 copy-start.2
  135.7 0.8 copy.33
  136.5 0.4 copy-done.2
  136.9 0.0 copy-start.4
  136.9 0.8 copy.34
  137.7 0.4 copy-done.4
  138.1 0.0 copy-start.3
  138.1 0.8 copy.35
  138.9 0.4 copy-done.3
  139.4 0.8 copy.36
  (3 shorter events, 0.0 us)
Async XLA Ops:
  0.7 0.7 copy-start.14
  0.7 0.7 copy-start.13
  0.7 1.5 %copy-start.8 = (f32[5,256]{1,0:T(8,128)S(1)}, f32[5,256]{1,0:T(8,128)}, u32[]{:S(2)}) copy-start(f32[5,256]{1,0:T(8,128)} %param.25) | copy-start | bytes 15364
  1.3 0.7 copy-start.12
  2.1 0.7 copy-start.10
  2.1 0.7 copy-start.11
  2.9 0.7 copy-start.9
  3.6 1.7 %copy-start.6 = (bf16[512,256]{1,0:T(8,128)(2,1)S(1)}, bf16[512,256]{1,0:T(8,128)(2,1)}, u32[]{:S(2)}) copy-start(bf16[512,256]{1,0:T(8,128)(2,1)} %param.18) | copy-start | bytes 786436
  4.2 1.1 copy-start.1
  5.3 0.8 copy-start
  6.1 1.0 copy-start.7
  133.7 1.9 %copy-start.5 = (bf16[128,2048]{1,0:T(8,128)(2,1)S(1)}, bf16[128,2048]{1,0:T(8,128)(2,1)}, u32[]{:S(2)}) copy-start(bf16[128,2048]{1,0:T(8,128)(2,1)} %get-tuple-element.29) | copy-start | bytes 1572868
  135.7 1.2 copy-start.2
  136.9 1.2 copy-start.4
  138.1 1.2 copy-start.3
where the time goes:
time: 142 us; the launch traced here: 140 us
  Pallas kernels  124 us (87%)
  local copies, waits for them, and re-layouts  13.5 us (10%)
  other arithmetic  1.73 us (1%)
    pallas_call x2, Pallas kernels, comm_call(): pl.pallas_call(kernel, in_specs=[vmem] * len(args), out_specs=[vmem] * le...  97.9 us
    pallas_call x1, Pallas kernels, mixer_backward(): pl.pallas_call(functools.partial(mixer_kernel, heads, tile), in_specs=[pl...  26.3 us
    unnamed x38, local copies, waits for them, and re-layouts  9.53 us

commit v1 on v0

v1 whole, which is shorter than its diff:
```python
import functools

import jax
import jax.numpy as jnp
from jax import lax
from jax.experimental import pallas as pl
from jax.experimental.pallas import tpu as pltpu
from jax.sharding import PartitionSpec as P

HEADS = 32
HEAD_DIM = 64
STATE = 128
GROUPS = 2
NORM_GROUPS = 8
CONV_K = 5
LANES = 128
HALO = 16
SKEW = 2
EPSILON = 1e-06
LOG2E = 1.4426950408889634
highest = lax.Precision.HIGHEST
f32 = jnp.float32
bf16 = jnp.bfloat16
NT = (((1,), (1,)), ((), ()))
TN = (((0,), (0,)), ((), ()))


def sigmoid(v):
    return 1.0 / (1.0 + jnp.exp(-v))


def softplus(v):
    e = jnp.exp(-jnp.abs(v))
    z = e / (2.0 + e)
    z2 = z * z
    series = jnp.full_like(z, 1.0 / 17.0)
    for odd in (15, 13, 11, 9, 7, 5, 3, 1):
        series = series * z2 + 1.0 / odd
    return jnp.maximum(v, 0.0) + 2.0 * z * series


def mm(a, b):
    return jnp.dot(a, b, preferred_element_type=f32)


def mm_nt(a, b):
    return lax.dot_general(a, b, NT, preferred_element_type=f32)


def mm_tn(a, b):
    return lax.dot_general(a, b, TN, preferred_element_type=f32)


def split_mm(a, b):
    hi = a.astype(bf16)
    lo = (a - hi.astype(f32)).astype(bf16)
    return mm(hi, b) + mm(lo, b)


def window_conv(rows, taps, count, flip):
    total = None
    for k in range(CONV_K):
        shift = HALO - CONV_K // 2 + k
        tap = taps[CONV_K - 1 - k if flip else k][None, :]
        term = tap * pltpu.roll(rows, rows.shape[0] - shift, axis=0)[:count]
        total = term if total is None else total + term
    return total


def greet(axes):
    barrier = pltpu.get_barrier_semaphore()
    count = 0
    for axis in axes:
        size = lax.axis_size(axis)
        me = lax.axis_index(axis)
        for o in range(1, size):
            pl.semaphore_signal(
                barrier,
                inc=1,
                device_id={axis: lax.rem(me + o, size)},
                device_id_type=pl.DeviceIdType.MESH,
            )
            count += 1
    pl.semaphore_wait(barrier, count)


def slot_table(sp, dp, cores, pairs):
    ny = dp // cores
    chunks = sp // GROUPS
    counts = (
        ("w_y", 2 * ny),
        ("w_core", 2),
        ("w_fwd", 2 * ny),
        ("la", dp),
        ("x", 1),
        ("x_left", GROUPS),
        ("x_right", GROUPS),
        ("dt", 1),
        ("drop", chunks),
        ("tap", sp),
        ("dy", NORM_GROUPS),
        ("bc", 1),
        ("bc_left", GROUPS),
        ("bc_right", GROUPS),
        ("right", pairs),
        ("left", pairs),
        ("gx", pairs),
        ("gx_left", GROUPS),
        ("gx_right", GROUPS),
        ("gbc", 1),
        ("gbc_left", GROUPS),
        ("gbc_right", GROUPS),
        ("ddt", 1),
        ("g_y", ny),
        ("g_core", 1),
        ("g_fwd", ny),
        ("w1", 2),
        ("w2", 2 * chunks),
        ("w3", 2 * chunks),
        ("w4", 2),
    )
    table = {}
    at = 0
    for name, count in counts:
        table[name] = at
        at += count
    return table, at


def mega_kernel(
    heads,
    cores,
    la_ref,
    wb_ref,
    wc_ref,
    x_ref,
    gates_ref,
    values_ref,
    adjoint_ref,
    dt_ref,
    drop_ref,
    tapx_ref,
    tapb_ref,
    tapc_ref,
    scale_ref,
    offset_ref,
    fade_ref,
    skip_ref,
    dgate_ref,
    dx_ref,
    ddt_ref,
    dh_ref,
    tall,
    wball,
    wcall,
    cols,
    xin,
    dyin,
    dysend,
    dtin,
    dropsend,
    dropin,
    drow,
    tapsend,
    tapin,
    tapall,
    bcsend,
    bcin,
    u_ref,
    sux_ref,
    dts_ref,
    ef_ref,
    eb_ref,
    tdec,
    vb_ref,
    vef_ref,
    veb_ref,
    dyef_ref,
    dyeb_ref,
    kn,
    rn,
    kt,
    rt,
    sbc_ref,
    score_ref,
    sign_ref,
    gesum,
    lcolb,
    lrow,
    sigrow,
    faderow,
    dv_ref,
    sr_ref,
    sl_ref,
    rin,
    lin,
    rout,
    lout,
    dksum,
    drsum,
    dlev,
    sdt,
    cross,
    colrow,
    dpx,
    gx,
    dpbc,
    gbc,
    ddtsend,
    gsend,
    gall,
    wsend,
    wown,
    w1in,
    s1send,
    w2in,
    s3send,
    ss,
    rs,
):
    dp = lax.axis_size("dp")
    sp = lax.axis_size("sp")
    me_dp = lax.axis_index("dp")
    me_sp = lax.axis_index("sp")
    ny = dp // cores
    chunks = sp // GROUPS
    y = me_dp // cores
    core = lax.rem(me_dp, cores)
    c = me_sp // GROUPS
    m = lax.rem(me_sp, GROUPS)
    p = GROUPS - 1 - m
    partner = c * GROUPS + p
    other_core = y * cores + (cores - 1 - core)
    tokens, inner = x_ref.shape
    gw = inner // GROUPS
    gh = HEADS // GROUPS
    ch = tokens * GROUPS
    pairs = gw // LANES
    cw = wb_ref.shape[0]
    latent = wb_ref.shape[1]
    xc = heads * HEAD_DIM
    nsrc = sp // GROUPS
    rows = cw // sp
    first = c == 0
    last = c == chunks - 1
    table, _ = slot_table(sp, dp, cores, pairs)
    sent = []

    def copy(src, dst, name, index, axis, peer, into=None):
        at = table[name]
        return pltpu.make_async_remote_copy(
            src_ref=src,
            dst_ref=dst,
            send_sem=ss.at[at + index],
            recv_sem=rs.at[at + (index if into is None else into)],
            device_id={axis: peer},
            device_id_type=pl.DeviceIdType.MESH,
        )

    def go(item, cond=None):
        if cond is None:
            item.start()
        else:

            @pl.when(cond)
            def _():
                item.start()

        sent.append((item, cond))
        return item

    def arrive(item, cond=None):
        if cond is None:
            item.wait_recv()
        else:

            @pl.when(cond)
            def _():
                item.wait_recv()

    def lanes(index, width):
        return pl.ds(pl.multiple_of(index * width, LANES), width)

    def near(step):
        return lax.rem(me_sp + step + 2 * sp, sp)

    mine = pl.ds(pl.multiple_of(HALO + m * tokens, HALO), tokens)
    mine0 = pl.ds(pl.multiple_of(m * tokens, HALO), tokens)
    body = slice(HALO, HALO + ch)
    left_rows = slice(0, HALO)
    right_rows = slice(HALO + ch, 2 * HALO + ch)
    to_right = jnp.logical_and(m == GROUPS - 1, jnp.logical_not(last))
    to_left = jnp.logical_and(m == 0, jnp.logical_not(first))

    greet(("dp", "sp"))

    w_y = []
    for o in range(1, ny):
        peer = lax.rem(y + o, ny) * cores + core
        w_y.append(
            (
                go(copy(wb_ref, wball.at[me_dp], "w_y", 2 * o, "dp", peer)),
                go(copy(wc_ref, wcall.at[me_dp], "w_y", 2 * o + 1, "dp", peer)),
            )
        )
    w_core = []
    if cores > 1:
        w_core = [
            go(copy(wb_ref, wball.at[me_dp], "w_core", 0, "dp", other_core)),
            go(copy(wc_ref, wcall.at[me_dp], "w_core", 1, "dp", other_core)),
        ]
    x_copy = go(copy(x_ref.at[:, lanes(p, gw)], xin.at[mine, :], "x", 0, "sp", partner))
    dt_copy = go(
        copy(
            dt_ref.at[pl.ds(pl.multiple_of(p * gh, gh), gh), :],
            dtin.at[:, lanes(m, tokens)],
            "dt",
            0,
            "sp",
            partner,
        )
    )

    def send_halo(name, source, target):
        for g in range(GROUPS):
            go(
                copy(
                    source(g, slice(tokens - HALO, tokens)),
                    target.at[left_rows, :],
                    name + "_left",
                    g,
                    "sp",
                    near(1 + g),
                    into=0,
                ),
                to_right,
            )
            go(
                copy(
                    source(g, slice(0, HALO)),
                    target.at[right_rows, :],
                    name + "_right",
                    g,
                    "sp",
                    near(g - GROUPS),
                    into=0,
                ),
                to_left,
            )

    def await_halo(name, target):
        arrive(
            copy(target.at[left_rows, :], target.at[left_rows, :], name + "_left", 0, "sp", partner),
            jnp.logical_not(first),
        )
        arrive(
            copy(target.at[right_rows, :], target.at[right_rows, :], name + "_right", 0, "sp", partner),
            jnp.logical_not(last),
        )

        @pl.when(first)
        def _():
            target[left_rows, :] = jnp.zeros((HALO, target.shape[1]), bf16)

        @pl.when(last)
        def _():
            target[right_rows, :] = jnp.zeros((HALO, target.shape[1]), bf16)

    send_halo("x", lambda g, r: x_ref.at[r, g * gw : (g + 1) * gw], xin)

    rows_h = dropsend.shape[1]
    head_row = lax.broadcasted_iota(jnp.int32, (rows_h, LANES), 0)
    offsets = jnp.zeros((rows_h, LANES), f32)
    fades = jnp.zeros((rows_h, LANES), f32)
    for h in range(heads):
        offsets = jnp.where(head_row == h, offset_ref[h], offsets)
        fades = jnp.where(head_row == h, fade_ref[h], fades)
    dropsend[...] = jnp.zeros_like(dropsend)
    for k in range(chunks):
        dropsend[k, :heads, :ch] = drop_ref[:, k * ch : (k + 1) * ch]
        dropsend[k, :, ch : ch + LANES] = offsets
        dropsend[k, :, ch + LANES :] = fades
    owner = (me_sp * heads) // gh
    place = me_sp - owner * nsrc
    for o in range(chunks):
        k = lax.rem(c + o, chunks)
        go(
            copy(
                dropsend.at[k],
                dropin.at[place],
                "drop",
                o,
                "sp",
                k * GROUPS + owner if o else partner,
                into=place,
            ),
            None if o else owner != m,
        )

    @pl.when(owner == m)
    def _():
        dropin[place] = dropsend[c]

    xw = tapsend.shape[1]
    tap_lane = lax.broadcasted_iota(jnp.int32, (1, xw), 1) // HEAD_DIM
    skips = jnp.zeros((1, xw), f32)
    for h in range(heads):
        skips = jnp.where(tap_lane == h, skip_ref[h], skips)
    tapsend[...] = jnp.zeros_like(tapsend)
    tapsend[:CONV_K, :xc] = tapx_ref[...]
    tapsend[CONV_K : CONV_K + 1, :] = skips
    tap_copies = []
    for o in range(1, sp):
        tap_copies.append(go(copy(tapsend, tapin.at[me_sp], "tap", o, "sp", lax.rem(me_sp + o, sp))))
    tapin[me_sp] = tapsend[...]
    la_copies = []
    for o in range(1, dp):
        peer = lax.rem(me_dp + o, dp)
        la_copies.append(
            go(copy(la_ref.at[:, lanes(peer, cw)], cols.at[me_dp], "la", o, "dp", peer))
        )
    cols[me_dp] = la_ref[:, lanes(me_dp, cw)]
    xin[mine, :] = x_ref[:, lanes(m, gw)]
    dtin[:, lanes(m, tokens)] = dt_ref[pl.ds(pl.multiple_of(m * gh, gh), gh), :]

    width = inner // NORM_GROUPS
    per_half = NORM_GROUPS // GROUPS
    dy_copies = []
    for half in range(GROUPS):
        who = p if half == 0 else m
        for i in range(per_half):
            span = lanes(who * per_half + i, width)
            values = values_ref[:, span].astype(f32)
            gates = gates_ref[:, span].astype(f32)
            sig = sigmoid(gates)
            act = gates * sig
            g = values * act
            dn = adjoint_ref[:, span].astype(f32) * scale_ref[:, span]
            inv = lax.rsqrt(jnp.sum(g * g, axis=1, keepdims=True) * (1.0 / width) + EPSILON)
            along = jnp.sum(dn * g, axis=1, keepdims=True) * (1.0 / width)
            dg = inv * dn - g * (inv * inv * inv * along)
            dgate_ref[:, span] = (dg * values * (sig + act * (1.0 - sig))).astype(bf16)
            dy = (dg * act).astype(bf16)
            at = slice(i * width, (i + 1) * width)
            if half == 0:
                dysend[:, at] = dy
                dy_copies.append(
                    go(copy(dysend.at[:, at], dyin.at[mine0, at], "dy", i, "sp", partner))
                )
            else:
                dyin[mine0, at] = dy

    arrive(dt_copy)
    for i in range(nsrc):
        arrive(
            copy(dropsend.at[0], dropin.at[i], "drop", i, "sp", partner), m * nsrc + i != me_sp
        )
        drow[i * heads : (i + 1) * heads, :] = dropin[i, :heads, :]
    twice = lambda v: jnp.concatenate([v] * (ch // LANES), axis=1)
    fade = jnp.exp(drow[:, ch + LANES :])
    a = dtin[...].astype(f32) + twice(drow[:, ch : ch + LANES])
    dt = softplus(a)
    sigrow[...] = sigmoid(a)
    faderow[...] = fade
    rate = dt * twice(fade) + drow[:, :ch]
    row_i = lax.broadcasted_iota(jnp.int32, (ch, ch), 0)
    col_i = lax.broadcasted_iota(jnp.int32, (ch, ch), 1)
    upper = (row_i <= col_i).astype(f32)
    level = jnp.dot(rate, upper, precision=highest, preferred_element_type=f32) * LOG2E
    lrow[...] = level
    fill = jnp.zeros((LANES - gh, ch), f32)
    lcol = jnp.concatenate([level, fill], axis=0).T
    dtcol = jnp.concatenate([dt, fill], axis=0).T
    low_lane = lax.broadcasted_iota(jnp.int32, (ch, LANES), 1) < HEAD_DIM
    for j in range(pairs):
        pair = []
        for h in (2 * j, 2 * j + 1):
            wide = jnp.broadcast_to(lcol[:, h : h + 1], (ch, LANES))
            lcolb[h] = wide
            pair.append(wide)
        spread = jnp.where(low_lane, pair[0], pair[1])
        end = spread[ch - 1 : ch, :]
        ef_ref[j] = jnp.exp2(-spread)
        eb_ref[j] = jnp.exp2(spread - end)
        tdec[j] = jnp.broadcast_to(jnp.exp2(-end), (8, LANES))
        dts_ref[j] = jnp.where(low_lane, dtcol[:, 2 * j : 2 * j + 1], dtcol[:, 2 * j + 1 : 2 * j + 2])

    for item in tap_copies:
        arrive(item)
    if xc % LANES == 0:
        for i in range(sp):
            tapall[:, i * xc : (i + 1) * xc] = tapin[i]
    else:
        per = LANES // xc
        for i in range(inner // LANES):
            tapall[:, i * LANES : (i + 1) * LANES] = jnp.concatenate(
                [tapin[i * per + q][:, :xc] for q in range(per)], axis=1
            )
    arrive(x_copy)
    await_halo("x", xin)

    @pl.loop(0, pairs)
    def _(j):
        taps = tapall[:, lanes(m * pairs + j, LANES)]
        pre = window_conv(xin[:, lanes(j, LANES)].astype(f32), taps, ch, False)
        sig = sigmoid(pre)
        u = pre * sig
        u_ref[j] = u
        sux_ref[j] = sig + u * (1.0 - sig)
        v = u * dts_ref[j]
        vb_ref[j] = v.astype(bf16)
        vef_ref[j] = (v * ef_ref[j]).astype(bf16)
        veb_ref[j] = (v * eb_ref[j]).astype(bf16)

    wball[me_dp] = wb_ref[...]
    wcall[me_dp] = wc_ref[...]

    def project(total, index):
        part = la_ref[:, lanes(index, cw)]
        tb, tc = mm(part, wball[index]), mm(part, wcall[index])
        return (tb, tc) if total is None else (total[0] + tb, total[1] + tc)

    total = project(None, me_dp)
    for item in w_core:
        arrive(item)
    if cores > 1:
        total = project(total, other_core)
    w_fwd = []
    for o in range(1, ny):
        src = lax.rem(y - o + ny, ny) * cores + core
        for q in range(2):
            arrive(w_y[o - 1][q])
            if cores > 1:
                full = (wball, wcall)[q].at[src]
                w_fwd.append(go(copy(full, full, "w_fwd", 2 * o + q, "dp", other_core)))
        total = project(total, src)
    for o in range(1, ny):
        if cores > 1:
            arrive(w_fwd[2 * o - 2])
            arrive(w_fwd[2 * o - 1])
            total = project(total, lax.rem(y - o + ny, ny) * cores + cores - 1 - core)
    proj_b, proj_c = total[0].astype(bf16), total[1].astype(bf16)
    for g in range(GROUPS):
        bcsend[g, :, :STATE] = proj_b[:, g * STATE : (g + 1) * STATE]
        bcsend[g, :, STATE:] = proj_c[:, g * STATE : (g + 1) * STATE]
    bc_copy = go(copy(bcsend.at[p], bcin.at[mine, :], "bc", 0, "sp", partner))
    send_halo("bc", lambda g, r: bcsend.at[g, r, :], bcin)
    bcin[mine, :] = bcsend[m]

    for item in dy_copies:
        arrive(item)

    @pl.loop(0, pairs)
    def _(j):
        dy = dyin[:, lanes(j, LANES)].astype(f32)
        dyef_ref[j] = (dy * ef_ref[j]).astype(bf16)
        dyeb_ref[j] = (dy * eb_ref[j]).astype(bf16)

    arrive(bc_copy)
    await_halo("bc", bcin)
    for q in range(2):
        taps = (tapb_ref, tapc_ref)[q][:, lanes(m, STATE)]
        at = slice(q * STATE, (q + 1) * STATE)
        pre = window_conv(bcin[:, at].astype(f32), taps, ch, False)
        sig = sigmoid(pre)
        kr = pre * sig
        sbc_ref[:, at] = sig + kr * (1.0 - sig)
        (kn, rn)[q][...] = kr.astype(bf16)
        (kt, rt)[q][...] = kr.T.astype(bf16)
    score = mm_nt(kn[...], rn[...])
    score_ref[...] = score
    sign_ref[...] = score * jnp.clip(col_i - row_i, -1, 1).astype(f32)

    gesum[...] = jnp.zeros_like(gesum)
    dksum[...] = jnp.zeros_like(dksum)
    drsum[...] = jnp.zeros_like(drsum)
    dlev[...] = jnp.zeros_like(dlev)
    sdt[...] = jnp.zeros_like(sdt)
    cross[...] = jnp.zeros_like(cross)

    @pl.when(first)
    def _():
        rin[...] = jnp.zeros_like(rin)

    @pl.when(last)
    def _():
        lin[...] = jnp.zeros_like(lin)

    lane_low = lax.broadcasted_iota(jnp.int32, (1, LANES), 1) < HEAD_DIM
    masks = (lane_low.astype(bf16), 1.0 - lane_low.astype(bf16))
    pick_lane = lax.broadcasted_iota(jnp.int32, (LANES, LANES), 1)
    pick_half = lax.broadcasted_iota(jnp.int32, (LANES, LANES), 0) // HEAD_DIM
    block = min(ch, LANES)

    def intra(j):
        dyj = dyin[:, lanes(j, LANES)]
        for a in range(2):
            h = 2 * j + a
            lr = lrow[pl.ds(h, 1), :]
            dym = dyj * masks[a]
            onehot = (pick_lane == h).astype(bf16)
            below = None
            for b in range(ch // block):
                at = slice(b * block, (b + 1) * block)
                gap = twice(lcolb[h, at]) - lr
                decay = jnp.exp2(-jnp.abs(gap))
                ge = mm_nt(vb_ref[j, at] * masks[a], dyj) * decay
                gesum[at, :] += ge
                part = mm((score_ref[at, :] * decay).astype(bf16), dym)
                if a == 0:
                    dv_ref[j, at] = part
                else:
                    dv_ref[j, at] += part
                q = sign_ref[at, :] * ge
                down = jnp.sum(q, axis=0, keepdims=True)
                below = down if below is None else below + down
                part = q[:, :LANES]
                for piece in range(1, ch // LANES):
                    part = part + q[:, piece * LANES : (piece + 1) * LANES]
                dlev[at, :] += split_mm(part, onehot)
            colrow[pl.ds(h, 1), :] = below

    def gx_copy(j):
        return copy(
            dpx.at[pl.ds(pl.multiple_of(p * (tokens - HALO), HALO), tokens + HALO), lanes(j, LANES)],
            gx.at[
                m, pl.ds(pl.multiple_of(HALO - HALO * p, HALO), tokens + HALO), lanes(j, LANES)
            ],
            "gx",
            j,
            "sp",
            partner,
        )

    keep_src = pl.ds(pl.multiple_of(m * (tokens - HALO), HALO), tokens + HALO)
    keep_dst = pl.ds(pl.multiple_of(HALO - HALO * m, HALO), tokens + HALO)

    def consume(j):
        k, r = kn[...], rn[...]
        ra, rb, la, lb = rin[j, 0], rin[j, 1], lin[j, 0], lin[j, 1]
        ef, eb = ef_ref[j], eb_ref[j]
        u = u_ref[j]
        at = lanes(j, LANES)
        dy = dyin[:, at].astype(f32)
        v = vb_ref[j].astype(f32)
        skip = tapall[CONV_K : CONV_K + 1, lanes(m * pairs + j, LANES)]
        onehot = (pick_lane == 2 * j + pick_half).astype(bf16)
        dl, dr = ef * mm(k, rb), eb * mm(k, lb)
        ml, mr = ef * mm(r, ra), eb * mm(r, la)
        dv = dv_ref[j] + dl + dr
        dpx[:, at] = ((dv * dts_ref[j] + skip * dy) * sux_ref[j]).astype(bf16)
        gx_copy(j).start()
        gx[m, keep_dst, at] = dpx[keep_src, at]
        dksum[...] += mm_nt(vef_ref[j], rb) + mm_nt(veb_ref[j], lb)
        drsum[...] += mm_nt(dyef_ref[j], ra) + mm_nt(dyeb_ref[j], la)
        dlev[...] += split_mm(dy * (mr - ml) + v * (dr - dl), onehot)
        sdt[...] += split_mm(u * dv, onehot)
        over = lb.astype(f32) * rout[j, 0].astype(f32) + la.astype(f32) * rout[j, 1].astype(f32)
        over = jnp.broadcast_to(jnp.sum(over, axis=0, keepdims=True), (8, LANES))
        cross[...] += split_mm(over, onehot)

    def chain(name, j, into_ref, own_ref, out_ref, head, tail, step):
        item = copy(out_ref.at[j], into_ref.at[j], name, j, "sp", near(step))

        @pl.when(jnp.logical_not(head))
        def _():
            item.wait_recv()

        decay = tdec[j][0:1, :]
        for q in range(2):
            out_ref[j, q] = (own_ref[j, q] + decay * into_ref[j, q].astype(f32)).astype(bf16)

        @pl.when(jnp.logical_not(tail))
        def _():
            item.start()

    delay = SKEW * (chunks - 1)

    @pl.loop(0, pairs + delay)
    def _(tick):
        @pl.when(tick < pairs)
        def _():
            sr_ref[tick, 0] = mm(kt[...], veb_ref[tick])
            sr_ref[tick, 1] = mm(rt[...], dyeb_ref[tick])
            sl_ref[tick, 0] = mm(kt[...], vef_ref[tick])
            sl_ref[tick, 1] = mm(rt[...], dyef_ref[tick])

        jr = tick - SKEW * c

        @pl.when(jnp.logical_and(jr >= 0, jr < pairs))
        def _():
            chain("right", jr, rin, sr_ref, rout, first, last, GROUPS)

        jl = tick - SKEW * (chunks - 1 - c)

        @pl.when(jnp.logical_and(jl >= 0, jl < pairs))
        def _():
            chain("left", jl, lin, sl_ref, lout, last, first, -GROUPS)

        @pl.when(tick < pairs)
        def _():
            intra(tick)

        @pl.when(tick == pairs - 1)
        def _():
            ge = gesum[...].astype(bf16)
            dksum[...] += mm(ge, rn[...])
            drsum[...] += mm_tn(ge, kn[...])

        @pl.when(tick >= delay)
        def _():
            consume(tick - delay)

    sbc = sbc_ref[...]
    dpbc[:, :STATE] = (dksum[...] * sbc[:, :STATE]).astype(bf16)
    dpbc[:, STATE:] = (drsum[...] * sbc[:, STATE:]).astype(bf16)
    gbc_copy = go(
        copy(
            dpbc.at[pl.ds(pl.multiple_of(p * (tokens - HALO), HALO), tokens + HALO), :],
            gbc.at[m, pl.ds(pl.multiple_of(HALO - HALO * p, HALO), tokens + HALO), :],
            "gbc",
            0,
            "sp",
            partner,
        )
    )

    def send_edges(name, source, target):
        go(
            copy(
                source.at[ch - HALO :, :],
                target.at[m, :HALO, :],
                name + "_left",
                0,
                "sp",
                lax.rem((c + 1) * GROUPS, sp),
                into=m,
            ),
            jnp.logical_not(last),
        )
        go(
            copy(
                source.at[:HALO, :],
                target.at[m, HALO + tokens :, :],
                name + "_right",
                0,
                "sp",
                lax.rem(c * GROUPS - 1 + sp, sp),
                into=m,
            ),
            jnp.logical_not(first),
        )

    def await_edges(name, target):
        lead, trail = m == 0, m == GROUPS - 1
        for g in range(GROUPS):
            slot = target.at[g, :HALO, :]
            arrive(
                copy(slot, slot, name + "_left", g, "sp", partner),
                jnp.logical_and(lead, jnp.logical_not(first)),
            )
            slot = target.at[g, HALO + tokens :, :]
            arrive(
                copy(slot, slot, name + "_right", g, "sp", partner),
                jnp.logical_and(trail, jnp.logical_not(last)),
            )

        @pl.when(jnp.logical_and(lead, first))
        def _():
            target[:, :HALO, :] = jnp.zeros((GROUPS, HALO, target.shape[2]), bf16)

        @pl.when(jnp.logical_and(trail, last))
        def _():
            target[:, HALO + tokens :, :] = jnp.zeros((GROUPS, HALO, target.shape[2]), bf16)

    send_edges("gbc", dpbc, gbc)
    send_edges("gx", dpx, gx)
    gbc[m, keep_dst, :] = dpbc[keep_src, :]

    fill = jnp.zeros((LANES - gh, ch), f32)
    down = jnp.concatenate([colrow[...], fill], axis=0).T
    drate = jnp.dot(upper, dlev[...] - down, precision=highest, preferred_element_type=f32)
    drate = (drate - cross[0:1, :]).T[:gh]
    ddt = ((drate * twice(faderow[...]) + sdt[...].T[:gh]) * sigrow[...]).astype(bf16)
    for g in range(GROUPS):
        ddtsend[g] = ddt[:, g * tokens : (g + 1) * tokens]
    group_rows = pl.ds(pl.multiple_of(m * gh, gh), gh)
    ddt_copy = go(copy(ddtsend.at[p], ddt_ref.at[group_rows, :], "ddt", 0, "sp", partner))
    ddt_ref[group_rows, :] = ddtsend[m]

    arrive(gbc_copy)
    await_edges("gbc", gbc)
    for g in range(GROUPS):
        for q in range(2):
            at = slice(g * STATE, (g + 1) * STATE)
            taps = (tapb_ref, tapc_ref)[q][:, at]
            part = gbc[g, :, q * STATE : (q + 1) * STATE].astype(f32)
            to = q * latent + g * STATE
            gsend[:, to : to + STATE] = window_conv(part, taps, tokens, True).astype(bf16)

    g_y = []
    for o in range(1, ny):
        peer = lax.rem(y + o, ny) * cores + core
        g_y.append(go(copy(gsend, gall.at[me_dp], "g_y", o, "dp", peer)))
    g_core = None
    if cores > 1:
        g_core = go(copy(gsend, gall.at[me_dp], "g_core", 0, "dp", other_core))
    gall[me_dp] = gsend[...]
    gb, gc = gsend[:, :latent], gsend[:, latent:]
    for i in range(dp):
        dh_ref[:, i * cw : (i + 1) * cw] = (mm_nt(gb, wball[i]) + mm_nt(gc, wcall[i])).astype(bf16)
    for item in la_copies:
        arrive(item)
    g_fwd = []
    for o in range(1, ny):
        src = lax.rem(y - o + ny, ny) * cores + core
        arrive(g_y[o - 1])
        if cores > 1:
            g_fwd.append(go(copy(gall.at[src], gall.at[src], "g_fwd", o, "dp", other_core)))
    if cores > 1:
        arrive(g_core)
    for item in g_fwd:
        arrive(item)

    w1 = []
    for q in range(2):
        total = None
        for i in range(dp):
            term = mm_tn(cols[i], gall[i, :, q * latent : (q + 1) * latent])
            total = term if total is None else total + term
        total = total.reshape(GROUPS, chunks, rows, latent)
        wsend[q] = total.astype(bf16)
        w1.append(go(copy(wsend.at[q, p], w1in.at[q], "w1", q, "sp", partner)))

    def input_gradient(g):
        @pl.loop(0, pairs)
        def _(j):
            taps = tapall[:, lanes(g * pairs + j, LANES)]
            part = gx[g, :, lanes(j, LANES)].astype(f32)
            dx_ref[:, lanes(g * pairs + j, LANES)] = window_conv(part, taps, tokens, True).astype(
                bf16
            )

    @pl.loop(0, pairs)
    def _(j):
        gx_copy(j).wait_recv()

    await_edges("gx", gx)
    w2 = []
    for q in range(2):
        arrive(w1[q])
        part = wsend[q, m].astype(f32) + w1in[q].astype(f32)
        s1send[q] = part.astype(bf16)
        for o in range(1, chunks):
            k = lax.rem(c + o, chunks)
            w2.append(
                go(
                    copy(
                        s1send.at[q, k],
                        w2in.at[q, c],
                        "w2",
                        q * chunks + o,
                        "sp",
                        k * GROUPS + m,
                    )
                )
            )
        wown[q] = s1send[q, c].astype(f32)
    input_gradient(0)
    w3 = []
    for q in range(2):
        share = wown[q]
        for o in range(1, chunks):
            arrive(w2[q * (chunks - 1) + o - 1])
            share = share + w2in[q, lax.rem(c - o + chunks, chunks)].astype(f32)
        s3send[q] = share.astype(bf16)
        tall[q, m, c] = s3send[q]
        for o in range(1, chunks):
            k = lax.rem(c + o, chunks)
            w3.append(
                go(
                    copy(
                        s3send.at[q],
                        tall.at[q, m, c],
                        "w3",
                        q * chunks + o,
                        "sp",
                        k * GROUPS + m,
                    )
                )
            )
    input_gradient(1)
    w4 = []
    for q in range(2):
        for o in range(1, chunks):
            arrive(w3[q * (chunks - 1) + o - 1])
        w4.append(go(copy(tall.at[q, m], tall.at[q, m], "w4", q, "sp", partner)))
    arrive(ddt_copy)
    for item in w4:
        arrive(item)

    @pl.loop(0, pairs)
    def _(j):
        gx_copy(j).wait_send()

        @pl.when(jnp.logical_not(last))
        def _():
            copy(rout.at[j], rin.at[j], "right", j, "sp", near(GROUPS)).wait_send()

        @pl.when(jnp.logical_not(first))
        def _():
            copy(lout.at[j], lin.at[j], "left", j, "sp", near(-GROUPS)).wait_send()

    for item, cond in sent:
        if cond is None:
            item.wait_send()
        else:

            @pl.when(cond)
            def _():
                item.wait_send()


def out_kernel(dgate, dx, dh, tall, dgate_out, dx_out, dh_out, dwb_out, dwc_out):
    dgate_out[...] = dgate[...]
    dx_out[...] = dx[...]
    dh_out[...] = dh[...]
    dwb_out[...] = tall[0].astype(f32).reshape(dwb_out.shape)
    dwc_out[...] = tall[1].astype(f32).reshape(dwc_out.shape)


def local(
    layer_activity,
    writer_matrix,
    reader_matrix,
    source_unfiltered,
    switch_raw_signal,
    saved_result,
    final_adjoint,
    delta_raw,
    extra_logdrop,
    source_filter_coefs,
    writer_filter_coefs,
    reader_filter_coefs,
    delta_offset,
    fading_exponents,
    direct_factor,
    rescale_factor,
):
    tokens, width_in = layer_activity.shape[1:]
    inner = source_unfiltered.shape[2]
    dp = lax.axis_size("dp")
    sp = lax.axis_size("sp")
    cores = 2 if dp % 2 == 0 else 1
    heads = delta_offset.shape[0]
    cw, latent = writer_matrix.shape
    xc = heads * HEAD_DIM
    xw = -(-xc // LANES) * LANES
    rows_h = -(-heads // 8) * 8
    chunks = sp // GROUPS
    ch = tokens * GROUPS
    gw = inner // GROUPS
    gh = HEADS // GROUPS
    pairs = gw // LANES
    rows = cw // sp
    window = tokens * sp
    _, slots = slot_table(sp, dp, cores, pairs)

    vmem = pl.BlockSpec(memory_space=pltpu.VMEM)
    smem = pl.BlockSpec(memory_space=pltpu.SMEM)
    scratch = [
        ((dp, cw, latent), bf16),
        ((dp, cw, latent), bf16),
        ((dp, tokens, cw), bf16),
        ((ch + 2 * HALO, gw), bf16),
        ((ch, gw), bf16),
        ((tokens, gw), bf16),
        ((gh, ch), bf16),
        ((chunks, rows_h, ch + 2 * LANES), f32),
        ((chunks, rows_h, ch + 2 * LANES), f32),
        ((gh, ch + 2 * LANES), f32),
        ((8, xw), f32),
        ((sp, 8, xw), f32),
        ((8, inner), f32),
        ((GROUPS, tokens, 2 * STATE), bf16),
        ((ch + 2 * HALO, 2 * STATE), bf16),
        ((pairs, ch, LANES), f32),
        ((pairs, ch, LANES), f32),
        ((pairs, ch, LANES), f32),
        ((pairs, ch, LANES), f32),
        ((pairs, ch, LANES), f32),
        ((pairs, 8, LANES), f32),
        ((pairs, ch, LANES), bf16),
        ((pairs, ch, LANES), bf16),
        ((pairs, ch, LANES), bf16),
        ((pairs, ch, LANES), bf16),
        ((pairs, ch, LANES), bf16),
        ((ch, STATE), bf16),
        ((ch, STATE), bf16),
        ((STATE, ch), bf16),
        ((STATE, ch), bf16),
        ((ch, 2 * STATE), f32),
        ((ch, ch), f32),
        ((ch, ch), f32),
        ((ch, ch), f32),
        ((gh, ch, LANES), f32),
        ((gh, ch), f32),
        ((gh, ch), f32),
        ((gh, LANES), f32),
        ((pairs, ch, LANES), f32),
        ((pairs, 2, STATE, LANES), f32),
        ((pairs, 2, STATE, LANES), f32),
        ((pairs, 2, STATE, LANES), bf16),
        ((pairs, 2, STATE, LANES), bf16),
        ((pairs, 2, STATE, LANES), bf16),
        ((pairs, 2, STATE, LANES), bf16),
        ((ch, STATE), f32),
        ((ch, STATE), f32),
        ((ch, LANES), f32),
        ((ch, LANES), f32),
        ((8, LANES), f32),
        ((gh, ch), f32),
        ((ch, gw), bf16),
        ((GROUPS, tokens + 2 * HALO, gw), bf16),
        ((ch, 2 * STATE), bf16),
        ((GROUPS, tokens + 2 * HALO, 2 * STATE), bf16),
        ((GROUPS, gh, tokens), bf16),
        ((tokens, 2 * latent), bf16),
        ((dp, tokens, 2 * latent), bf16),
        ((2, GROUPS, chunks, rows, latent), bf16),
        ((2, rows, latent), f32),
        ((2, chunks, rows, latent), bf16),
        ((2, chunks, rows, latent), bf16),
        ((2, chunks, rows, latent), bf16),
        ((2, rows, latent), bf16),
    ]
    dgate, dx, ddt, dh, tall = pl.pallas_call(
        functools.partial(mega_kernel, heads, cores),
        in_specs=[vmem] * 13 + [smem] * 3,
        out_specs=[vmem] * 5,
        out_shape=[
            jax.ShapeDtypeStruct((tokens, inner), bf16),
            jax.ShapeDtypeStruct((tokens, inner), bf16),
            jax.ShapeDtypeStruct((HEADS, tokens), bf16),
            jax.ShapeDtypeStruct((tokens, width_in), bf16),
            jax.ShapeDtypeStruct((2, GROUPS, chunks, rows, latent), bf16),
        ],
        scratch_shapes=[pltpu.VMEM(shape, kind) for shape, kind in scratch]
        + [pltpu.SemaphoreType.DMA((slots,)), pltpu.SemaphoreType.DMA((slots,))],
        compiler_params=pltpu.CompilerParams(
            collective_id=0, has_side_effects=True, vmem_limit_bytes=60 * 1024 * 1024
        ),
        name="mega",
    )(
        layer_activity.reshape(tokens, width_in),
        writer_matrix,
        reader_matrix,
        source_unfiltered.reshape(tokens, inner),
        switch_raw_signal.reshape(tokens, inner),
        saved_result.reshape(tokens, inner),
        final_adjoint.reshape(tokens, inner),
        delta_raw.reshape(tokens, HEADS).T,
        extra_logdrop.reshape(window, heads).T,
        source_filter_coefs,
        writer_filter_coefs,
        reader_filter_coefs,
        rescale_factor.reshape(1, inner),
        delta_offset,
        fading_exponents,
        direct_factor,
    )
    d_gate, d_x, d_hidden, d_w_b, d_w_c = pl.pallas_call(
        out_kernel,
        in_specs=[vmem] * 4,
        out_specs=[vmem] * 5,
        out_shape=[
            jax.ShapeDtypeStruct((tokens, inner), bf16),
            jax.ShapeDtypeStruct((tokens, inner), bf16),
            jax.ShapeDtypeStruct((tokens, width_in), bf16),
            jax.ShapeDtypeStruct((cw, latent), f32),
            jax.ShapeDtypeStruct((cw, latent), f32),
        ],
        name="outputs",
    )(dgate, dx, dh, tall)
    return (
        d_hidden.reshape(1, tokens, width_in),
        d_x.reshape(1, tokens, inner),
        d_gate.reshape(1, tokens, inner),
        ddt.T.reshape(1, tokens, HEADS),
        d_w_b,
        d_w_c,
    )


def solution(mesh):
    in_specs = (
        P("dp", "sp", None),
        P("dp", None),
        P("dp", None),
        P("dp", "sp", None),
        P("dp", "sp", None),
        P("dp", "sp", None),
        P("dp", "sp", None),
        P("dp", "sp", None),
        P("dp", None, "sp"),
        P(None, "sp"),
        P(),
        P(),
        P("sp"),
        P("sp"),
        P("sp"),
        P(),
    )
    out_specs = (
        P("dp", "sp", None),
        P("dp", "sp", None),
        P("dp", "sp", None),
        P("dp", "sp", None),
        P("dp", None),
        P("dp", None),
    )
    return jax.shard_map(local, mesh=mesh, in_specs=in_specs, out_specs=out_specs, check_vma=False)
```

time: 142 us -> 88.2 us (0.62); the launches traced: 140 us -> 88 us
  Pallas kernels: 124 us -> 86.1 us
  local copies, waits for them, and re-layouts: 13.5 us -> 1.29 us
  other arithmetic: 1.73 us -> 0 us
    pallas_call x3 -> x2, Pallas kernels: 124 us -> 86.1 us  [the longest x1 83 us: local(): pl.pallas_call(functools.partial(mega_kernel, heads, cores), in_specs=[vm...]
    unnamed x38 -> x3, local copies, waits for them, and re-layouts: 9.53 us -> 1.29 us
    pad x2 -> x0, local copies, waits for them, and re-layouts: 1.46 us -> none  [the longest x1 0.84 us: pad_last(): return jnp.pad(values, pads)]
where the time goes in v1:
time: 88.2 us; the launch traced here: 88 us
  Pallas kernels  86.1 us (98%)
  local copies, waits for them, and re-layouts  1.29 us (1%)
    pallas_call x1, Pallas kernels, local(): pl.pallas_call(functools.partial(mega_kernel, heads, cores), in_specs=[vm...  83 us
    pallas_call x1, Pallas kernels, local(): pl.pallas_call(out_kernel, in_specs=[vmem] * 4, out_specs=[vmem] * 5, out...  3.04 us

profile of v1, /device:TPU:0, one launch (start us, length us, event | category | flops | bytes accessed | tf_op | source)
XLA Modules:
  0.0 88.0 jit_solution(1728037880102336673)
XLA Ops:
  0.6 83.0 %mega.1 = (bf16[128,2048]{1,0:T(8,128)(2,1)}, bf16[128,2048]{1,0:T(8,128)(2,1)}, bf16[32,128]{1,0:T(8,128)(2,1)}, bf16[128,2048]{1,0:T(8,128)(2,1)}, bf16[2,2,4,64,256]{4,3,2,1,0:T(8,128)(2,1)}) custom-call(bf16[128,2048]{1,0:T(8,128)(2,1)} %bitcast.18, bf16[512,256]{1,0:T(8,128)(2,1)} %wb_ref.1, bf16[512,256]{1,0:T(8,128)(2,1)} %wc_ref.1, ...), custom_call_target="tpu_custom_call" | custom-call | tf_op jit(solution)/shard_map/mega/pallas_call | solution.py:1037
  83.7 3.0 %outputs.1 = (bf16[128,2048]{1,0:T(8,128)(2,1)}, bf16[128,2048]{1,0:T(8,128)(2,1)}, bf16[128,2048]{1,0:T(8,128)(2,1)}, f32[512,256]{1,0:T(8,128)}, f32[512,256]{1,0:T(8,128)}) custom-call(bf16[128,2048]{1,0:T(8,128)(2,1)} %get-tuple-element.16.dgate, bf16[128,2048]{1,0:T(8,128)(2,1)} %get-tuple-element.17.dx, bf16[128,2048]{1,0:T(8,128)(2,1)} %get-tuple-element.18.dh, ...), custom_call_target="tpu_custom_call" | custom-call | tf_op jit(solution)/shard_map/outputs/pallas_call | solution.py:1072
  86.7 0.0 copy-start
  86.7 0.7 copy-done
  87.4 0.6 copy.23
Async XLA Ops:
  86.7 0.7 copy-start

commit v2 on v1

--- a/solution.py
+++ b/solution.py
@@ -82,6 +82,21 @@
             )
             count += 1
     pl.semaphore_wait(barrier, count)
+
+
+class Phases:
+    def __init__(self):
+        self.scope = None
+
+    def __call__(self, name):
+        self.end()
+        self.scope = jax.named_scope(name)
+        self.scope.__enter__()
+
+    def end(self):
+        if self.scope is not None:
+            self.scope.__exit__(None, None, None)
+            self.scope = None
 
 
 def slot_table(sp, dp, cores, pairs):
@@ -102,8 +117,8 @@
         ("bc", 1),
         ("bc_left", GROUPS),
         ("bc_right", GROUPS),
-        ("right", pairs),
-        ("left", pairs),
+        ("right", 2 * pairs),
+        ("left", 2 * pairs),
         ("gx", pairs),
         ("gx_left", GROUPS),
         ("gx_right", GROUPS),
@@ -111,9 +126,9 @@
         ("gbc_left", GROUPS),
         ("gbc_right", GROUPS),
         ("ddt", 1),
-        ("g_y", ny),
-        ("g_core", 1),
-        ("g_fwd", ny),
+        ("g_y", 2 * ny),
+        ("g_core", 2),
+        ("g_fwd", 2 * ny),
         ("w1", 2),
         ("w2", 2 * chunks),
         ("w3", 2 * chunks),
@@ -130,13 +145,13 @@
 def mega_kernel(
     heads,
     cores,
-    la_ref,
-    wb_ref,
-    wc_ref,
-    x_ref,
-    gates_ref,
-    values_ref,
-    adjoint_ref,
+    la_hbm,
+    wb_hbm,
+    wc_hbm,
+    x_hbm,
+    gates_hbm,
+    values_hbm,
+    adjoint_hbm,
     dt_ref,
     drop_ref,
     tapx_ref,
@@ -151,6 +166,13 @@
     ddt_ref,
     dh_ref,
     tall,
+    la_ref,
+    wb_ref,
+    wc_ref,
+    x_ref,
+    gates_ref,
+    values_ref,
+    adjoint_ref,
     wball,
     wcall,
     cols,
@@ -217,6 +239,7 @@
     s3send,
     ss,
     rs,
+    ls,
 ):
     dp = lax.axis_size("dp")
     sp = lax.axis_size("sp")
@@ -292,8 +315,27 @@
     to_right = jnp.logical_and(m == GROUPS - 1, jnp.logical_not(last))
     to_left = jnp.logical_and(m == 0, jnp.logical_not(first))
 
+    phase = Phases()
+    phase("greet")
+    loads = {}
+    for at, (source, target) in enumerate(
+        (
+            (wb_hbm, wb_ref),
+            (wc_hbm, wc_ref),
+            (x_hbm, x_ref),
+            (values_hbm, values_ref),
+            (gates_hbm, gates_ref),
+            (adjoint_hbm, adjoint_ref),
+            (la_hbm, la_ref),
+        )
+    ):
+        loads[at] = pltpu.make_async_copy(source, target, ls.at[at])
+        loads[at].start()
     greet(("dp", "sp"))
-
+    loads[0].wait()
+    loads[1].wait()
+
+    phase("send_first")
     w_y = []
     for o in range(1, ny):
         peer = lax.rem(y + o, ny) * cores + core
@@ -309,6 +351,7 @@
             go(copy(wb_ref, wball.at[me_dp], "w_core", 0, "dp", other_core)),
             go(copy(wc_ref, wcall.at[me_dp], "w_core", 1, "dp", other_core)),
         ]
+    loads[2].wait()
     x_copy = go(copy(x_ref.at[:, lanes(p, gw)], xin.at[mine, :], "x", 0, "sp", partner))
     dt_copy = go(
         copy(
@@ -368,6 +411,7 @@
 
     send_halo("x", lambda g, r: x_ref.at[r, g * gw : (g + 1) * gw], xin)
 
+    phase("params")
     rows_h = dropsend.shape[1]
     head_row = lax.broadcasted_iota(jnp.int32, (rows_h, LANES), 0)
     offsets = jnp.zeros((rows_h, LANES), f32)
@@ -413,6 +457,7 @@
     for o in range(1, sp):
         tap_copies.append(go(copy(tapsend, tapin.at[me_sp], "tap", o, "sp", lax.rem(me_sp + o, sp))))
     tapin[me_sp] = tapsend[...]
+    loads[6].wait()
     la_copies = []
     for o in range(1, dp):
         peer = lax.rem(me_dp + o, dp)
@@ -423,9 +468,12 @@
     xin[mine, :] = x_ref[:, lanes(m, gw)]
     dtin[:, lanes(m, tokens)] = dt_ref[pl.ds(pl.multiple_of(m * gh, gh), gh), :]
 
+    phase("norm")
     width = inner // NORM_GROUPS
     per_half = NORM_GROUPS // GROUPS
     dy_copies = []
+    for at in (3, 4, 5):
+        loads[at].wait()
     for half in range(GROUPS):
         who = p if half == 0 else m
         for i in range(per_half):
@@ -450,6 +498,7 @@
             else:
                 dyin[mine0, at] = dy
 
+    phase("levels")
     arrive(dt_copy)
     for i in range(nsrc):
         arrive(
@@ -485,6 +534,7 @@
         tdec[j] = jnp.broadcast_to(jnp.exp2(-end), (8, LANES))
         dts_ref[j] = jnp.where(low_lane, dtcol[:, 2 * j : 2 * j + 1], dtcol[:, 2 * j + 1 : 2 * j + 2])
 
+    phase("wait_x")
     for item in tap_copies:
         arrive(item)
     if xc % LANES == 0:
@@ -499,6 +549,7 @@
     arrive(x_copy)
     await_halo("x", xin)
 
+    phase("prep_x")
     @pl.loop(0, pairs)
     def _(j):
         taps = tapall[:, lanes(m * pairs + j, LANES)]
@@ -512,6 +563,7 @@
         vef_ref[j] = (v * ef_ref[j]).astype(bf16)
         veb_ref[j] = (v * eb_ref[j]).astype(bf16)
 
+    phase("project")
     wball[me_dp] = wb_ref[...]
     wcall[me_dp] = wc_ref[...]
 
@@ -547,6 +599,7 @@
     send_halo("bc", lambda g, r: bcsend.at[g, r, :], bcin)
     bcin[mine, :] = bcsend[m]
 
+    phase("wait_dy")
     for item in dy_copies:
         arrive(item)
 
@@ -556,8 +609,10 @@
         dyef_ref[j] = (dy * ef_ref[j]).astype(bf16)
         dyeb_ref[j] = (dy * eb_ref[j]).astype(bf16)
 
+    phase("wait_bc")
     arrive(bc_copy)
     await_halo("bc", bcin)
+    phase("conv_bc")
     for q in range(2):
         taps = (tapb_ref, tapc_ref)[q][:, lanes(m, STATE)]
         at = slice(q * STATE, (q + 1) * STATE)
@@ -649,7 +704,11 @@
         ml, mr = ef * mm(r, ra), eb * mm(r, la)
         dv = dv_ref[j] + dl + dr
         dpx[:, at] = ((dv * dts_ref[j] + skip * dy) * sux_ref[j]).astype(bf16)
-        gx_copy(j).start()
+
+        @pl.when(j < pairs - 1)
+        def _():
+            gx_copy(j).start()
+
         gx[m, keep_dst, at] = dpx[keep_src, at]
         dksum[...] += mm_nt(vef_ref[j], rb) + mm_nt(veb_ref[j], lb)
         drsum[...] += mm_nt(dyef_ref[j], ra) + mm_nt(dyeb_ref[j], la)
@@ -659,23 +718,27 @@
         over = jnp.broadcast_to(jnp.sum(over, axis=0, keepdims=True), (8, LANES))
         cross[...] += split_mm(over, onehot)
 
+    def chain_copy(name, j, q, into_ref, out_ref, step):
+        return copy(out_ref.at[j, q], into_ref.at[j, q], name, 2 * j + q, "sp", near(step))
+
     def chain(name, j, into_ref, own_ref, out_ref, head, tail, step):
-        item = copy(out_ref.at[j], into_ref.at[j], name, j, "sp", near(step))
-
-        @pl.when(jnp.logical_not(head))
-        def _():
-            item.wait_recv()
-
         decay = tdec[j][0:1, :]
         for q in range(2):
+            item = chain_copy(name, j, q, into_ref, out_ref, step)
+
+            @pl.when(jnp.logical_not(head))
+            def _():
+                item.wait_recv()
+
             out_ref[j, q] = (own_ref[j, q] + decay * into_ref[j, q].astype(f32)).astype(bf16)
 
-        @pl.when(jnp.logical_not(tail))
-        def _():
-            item.start()
+            @pl.when(jnp.logical_not(tail))
+            def _():
+                item.start()
 
     delay = SKEW * (chunks - 1)
 
+    phase("ticks")
     @pl.loop(0, pairs + delay)
     def _(tick):
         @pl.when(tick < pairs)
@@ -689,17 +752,20 @@
 
         @pl.when(jnp.logical_and(jr >= 0, jr < pairs))
         def _():
-            chain("right", jr, rin, sr_ref, rout, first, last, GROUPS)
+            with jax.named_scope("chain_r"):
+                chain("right", jr, rin, sr_ref, rout, first, last, GROUPS)
 
         jl = tick - SKEW * (chunks - 1 - c)
 
         @pl.when(jnp.logical_and(jl >= 0, jl < pairs))
         def _():
-            chain("left", jl, lin, sl_ref, lout, last, first, -GROUPS)
+            with jax.named_scope("chain_l"):
+                chain("left", jl, lin, sl_ref, lout, last, first, -GROUPS)
 
         @pl.when(tick < pairs)
         def _():
-            intra(tick)
+            with jax.named_scope("intra"):
+                intra(tick)
 
         @pl.when(tick == pairs - 1)
         def _():
@@ -709,8 +775,10 @@
 
         @pl.when(tick >= delay)
         def _():
-            consume(tick - delay)
-
+            with jax.named_scope("consume"):
+                consume(tick - delay)
+
+    phase("send_dbc")
     sbc = sbc_ref[...]
     dpbc[:, :STATE] = (dksum[...] * sbc[:, :STATE]).astype(bf16)
     dpbc[:, STATE:] = (drsum[...] * sbc[:, STATE:]).astype(bf16)
@@ -774,9 +842,11 @@
             target[:, HALO + tokens :, :] = jnp.zeros((GROUPS, HALO, target.shape[2]), bf16)
 
     send_edges("gbc", dpbc, gbc)
+    gx_copy(pairs - 1).start()
     send_edges("gx", dpx, gx)
     gbc[m, keep_dst, :] = dpbc[keep_src, :]
 
+    phase("ddt")
     fill = jnp.zeros((LANES - gh, ch), f32)
     down = jnp.concatenate([colrow[...], fill], axis=0).T
     drate = jnp.dot(upper, dlev[...] - down, precision=highest, preferred_element_type=f32)
@@ -788,8 +858,10 @@
     ddt_copy = go(copy(ddtsend.at[p], ddt_ref.at[group_rows, :], "ddt", 0, "sp", partner))
     ddt_ref[group_rows, :] = ddtsend[m]
 
+    phase("wait_gbc")
     arrive(gbc_copy)
     await_edges("gbc", gbc)
+    phase("conv_g")
     for g in range(GROUPS):
         for q in range(2):
             at = slice(g * STATE, (g + 1) * STATE)
@@ -798,35 +870,58 @@
             to = q * latent + g * STATE
             gsend[:, to : to + STATE] = window_conv(part, taps, tokens, True).astype(bf16)
 
-    g_y = []
-    for o in range(1, ny):
-        peer = lax.rem(y + o, ny) * cores + core
-        g_y.append(go(copy(gsend, gall.at[me_dp], "g_y", o, "dp", peer)))
-    g_core = None
-    if cores > 1:
-        g_core = go(copy(gsend, gall.at[me_dp], "g_core", 0, "dp", other_core))
+    phase("d_hidden")
+    halves = [slice(q * latent, (q + 1) * latent) for q in range(2)]
+
+    def g_copy(source, block, name, index, q, peer):
+        return go(
+            copy(
+                source.at[:, halves[q]],
+                gall.at[block, :, halves[q]],
+                name,
+                2 * index + q,
+                "dp",
+                peer,
+            )
+        )
+
+    g_y = {}
+    g_core = {}
+    for q in range(2):
+        for o in range(1, ny):
+            peer = lax.rem(y + o, ny) * cores + core
+            g_y[o, q] = g_copy(gsend, me_dp, "g_y", o, q, peer)
+        if cores > 1:
+            g_core[q] = g_copy(gsend, me_dp, "g_core", 0, q, other_core)
     gall[me_dp] = gsend[...]
     gb, gc = gsend[:, :latent], gsend[:, latent:]
     for i in range(dp):
         dh_ref[:, i * cw : (i + 1) * cw] = (mm_nt(gb, wball[i]) + mm_nt(gc, wcall[i])).astype(bf16)
+    phase("wait_g")
     for item in la_copies:
         arrive(item)
-    g_fwd = []
-    for o in range(1, ny):
-        src = lax.rem(y - o + ny, ny) * cores + core
-        arrive(g_y[o - 1])
+    w1 = []
+    g_fwd = {}
+
+    def forward_g(q):
+        for o in range(1, ny):
+            src = lax.rem(y - o + ny, ny) * cores + core
+            arrive(g_y[o, q])
+            if cores > 1:
+                g_fwd[o, q] = g_copy(gall.at[src], src, "g_fwd", o, q, other_core)
+
+    forward_g(0)
+    for q in range(2):
         if cores > 1:
-            g_fwd.append(go(copy(gall.at[src], gall.at[src], "g_fwd", o, "dp", other_core)))
-    if cores > 1:
-        arrive(g_core)
-    for item in g_fwd:
-        arrive(item)
-
-    w1 = []
-    for q in range(2):
+            arrive(g_core[q])
+            for o in range(1, ny):
+                arrive(g_fwd[o, q])
+        if q == 0:
+            forward_g(1)
+        phase("dw")
         total = None
         for i in range(dp):
-            term = mm_tn(cols[i], gall[i, :, q * latent : (q + 1) * latent])
+            term = mm_tn(cols[i], gall[i, :, halves[q]])
             total = term if total is None else total + term
         total = total.reshape(GROUPS, chunks, rows, latent)
         wsend[q] = total.astype(bf16)
@@ -841,11 +936,13 @@
                 bf16
             )
 
+    phase("wait_gx")
     @pl.loop(0, pairs)
     def _(j):
         gx_copy(j).wait_recv()
 
     await_edges("gx", gx)
+    phase("w2")
     w2 = []
     for q in range(2):
         arrive(w1[q])
@@ -866,7 +963,9 @@
                 )
             )
         wown[q] = s1send[q, c].astype(f32)
+    phase("dx0")
     input_gradient(0)
+    phase("w3")
     w3 = []
     for q in range(2):
         share = wown[q]
@@ -889,12 +988,15 @@
                     )
                 )
             )
+    phase("dx1")
     input_gradient(1)
+    phase("w4")
     w4 = []
     for q in range(2):
         for o in range(1, chunks):
             arrive(w3[q * (chunks - 1) + o - 1])
         w4.append(go(copy(tall.at[q, m], tall.at[q, m], "w4", q, "sp", partner)))
+    phase("last")
     arrive(ddt_copy)
     for item in w4:
         arrive(item)
@@ -905,11 +1007,13 @@
 
         @pl.when(jnp.logical_not(last))
         def _():
-            copy(rout.at[j], rin.at[j], "right", j, "sp", near(GROUPS)).wait_send()
+            for q in range(2):
+                chain_copy("right", j, q, rin, rout, GROUPS).wait_send()
 
         @pl.when(jnp.logical_not(first))
         def _():
-            copy(lout.at[j], lin.at[j], "left", j, "sp", near(-GROUPS)).wait_send()
+            for q in range(2):
+                chain_copy("left", j, q, lin, lout, -GROUPS).wait_send()
 
     for item, cond in sent:
         if cond is None:
@@ -920,8 +1024,11 @@
             def _():
                 item.wait_send()
 
-
-def out_kernel(dgate, dx, dh, tall, dgate_out, dx_out, dh_out, dwb_out, dwc_out):
+    phase.end()
+
+
+def out_kernel(dgate, dx, dh, ddt, tall, dgate_out, dx_out, dh_out, ddt_out, dwb_out, dwc_out):
+    ddt_out[...] = ddt[...]
     dgate_out[...] = dgate[...]
     dx_out[...] = dx[...]
     dh_out[...] = dh[...]
@@ -967,8 +1074,16 @@
     _, slots = slot_table(sp, dp, cores, pairs)
 
     vmem = pl.BlockSpec(memory_space=pltpu.VMEM)
+    hbm = pl.BlockSpec(memory_space=pltpu.HBM)
     smem = pl.BlockSpec(memory_space=pltpu.SMEM)
     scratch = [
+        ((tokens, width_in), bf16),
+        ((cw, latent), bf16),
+        ((cw, latent), bf16),
+        ((tokens, inner), bf16),
+        ((tokens, inner), bf16),
+        ((tokens, inner), bf16),
+        ((tokens, inner), bf16),
         ((dp, cw, latent), bf16),
         ((dp, cw, latent), bf16),
         ((dp, tokens, cw), bf16),
@@ -1036,17 +1151,18 @@
     ]
     dgate, dx, ddt, dh, tall = pl.pallas_call(
         functools.partial(mega_kernel, heads, cores),
-        in_specs=[vmem] * 13 + [smem] * 3,
+        in_specs=[hbm] * 7 + [vmem] * 6 + [smem] * 3,
         out_specs=[vmem] * 5,
         out_shape=[
-            jax.ShapeDtypeStruct((tokens, inner), bf16),
-            jax.ShapeDtypeStruct((tokens, inner), bf16),
-            jax.ShapeDtypeStruct((HEADS, tokens), bf16),
-            jax.ShapeDtypeStruct((tokens, width_in), bf16),
-            jax.ShapeDtypeStruct((2, GROUPS, chunks, rows, latent), bf16),
+            pltpu.VMEM((tokens, inner), bf16),
+            pltpu.VMEM((tokens, inner), bf16),
+            pltpu.VMEM((HEADS, tokens), bf16),
+            pltpu.VMEM((tokens, width_in), bf16),
+            pltpu.VMEM((2, GROUPS, chunks, rows, latent), bf16),
         ],
         scratch_shapes=[pltpu.VMEM(shape, kind) for shape, kind in scratch]
-        + [pltpu.SemaphoreType.DMA((slots,)), pltpu.SemaphoreType.DMA((slots,))],
+        + [pltpu.SemaphoreType.DMA((slots,)), pltpu.SemaphoreType.DMA((slots,))]
+        + [pltpu.SemaphoreType.DMA((7,))],
         compiler_params=pltpu.CompilerParams(
             collective_id=0, has_side_effects=True, vmem_limit_bytes=60 * 1024 * 1024
         ),
@@ -1069,24 +1185,25 @@
         fading_exponents,
         direct_factor,
     )
-    d_gate, d_x, d_hidden, d_w_b, d_w_c = pl.pallas_call(
+    d_gate, d_x, d_hidden, d_dt, d_w_b, d_w_c = pl.pallas_call(
         out_kernel,
-        in_specs=[vmem] * 4,
-        out_specs=[vmem] * 5,
+        in_specs=[vmem] * 5,
+        out_specs=[vmem] * 6,
         out_shape=[
             jax.ShapeDtypeStruct((tokens, inner), bf16),
             jax.ShapeDtypeStruct((tokens, inner), bf16),
             jax.ShapeDtypeStruct((tokens, width_in), bf16),
+            jax.ShapeDtypeStruct((HEADS, tokens), bf16),
             jax.ShapeDtypeStruct((cw, latent), f32),
             jax.ShapeDtypeStruct((cw, latent), f32),
         ],
         name="outputs",
-    )(dgate, dx, dh, tall)
+    )(*[pltpu.with_memory_space_constraint(v, pltpu.VMEM) for v in (dgate, dx, dh, ddt, tall)])
     return (
         d_hidden.reshape(1, tokens, width_in),
         d_x.reshape(1, tokens, inner),
         d_gate.reshape(1, tokens, inner),
-        ddt.T.reshape(1, tokens, HEADS),
+        d_dt.T.reshape(1, tokens, HEADS),
         d_w_b,
         d_w_c,
     )

time: 88.2 us -> 83.5 us (0.947)
  Pallas kernels: 86.1 us -> 82.7 us
  local copies, waits for them, and re-layouts: 1.29 us -> 0 us
    pallas_call x2, Pallas kernels: 86.1 us -> 82.7 us  [the longest x1 81 us: local(): pl.pallas_call(functools.partial(mega_kernel, heads, cores), in_specs=[hb...]
    unnamed x3 -> x0, local copies, waits for them, and re-layouts: 1.29 us -> none
where the time goes in v2:
time: 83.5 us; the launch traced here: 83.3 us
  Pallas kernels  82.7 us (99%)
    pallas_call x1, Pallas kernels, local(): pl.pallas_call(functools.partial(mega_kernel, heads, cores), in_specs=[hb...  81 us

profile of v2, /device:TPU:0, one launch (start us, length us, event | category | flops | bytes accessed | tf_op | source)
XLA Modules:
  0.0 83.3 jit_solution(7861932774615475080)
XLA Ops:
  0.6 81.0 %mega.1 = (bf16[128,2048]{1,0:T(8,128)(2,1)S(1)}, bf16[128,2048]{1,0:T(8,128)(2,1)S(1)}, bf16[32,128]{1,0:T(8,128)(2,1)S(1)}, bf16[128,2048]{1,0:T(8,128)(2,1)S(1)}, bf16[2,2,4,64,256]{4,3,2,1,0:T(8,128)(2,1)S(1)}) custom-call(bf16[128,2048]{1,0:T(8,128)(2,1)} %bitcast.18, bf16[512,256]{1,0:T(8,128)(2,1)} %wb_hbm.1, bf16[512,256]{1,0:T(8,128)(2,1)} %wc_hbm.1, ...), custom_call_target="tpu_custom_call" | custom-call | tf_op jit(solution)/shard_map/mega/pallas_call | solution.py:1152
  81.7 1.6 %outputs.1 = (bf16[128,2048]{1,0:T(8,128)(2,1)}, bf16[128,2048]{1,0:T(8,128)(2,1)}, bf16[128,2048]{1,0:T(8,128)(2,1)}, bf16[32,128]{1,0:T(8,128)(2,1)}, f32[512,256]{1,0:T(8,128)}, /*index=5*/f32[512,256]{1,0:T(8,128)}) custom-call(bf16[128,2048]{1,0:T(8,128)(2,1)S(1)} %get-tuple-element.17.dgate, bf16[128,2048]{1,0:T(8,128)(2,1)S(1)} %get-tuple-element.18.dx, ...), custom_call_target="tpu_custom_call" | custom-call | tf_op jit(solution)/shard_map/outputs/pallas_call | solution.py:1188

commit v3 on v2

--- a/solution.py
+++ b/solution.py
@@ -106,7 +106,9 @@
         ("w_y", 2 * ny),
         ("w_core", 2),
         ("w_fwd", 2 * ny),
-        ("la", dp),
+        ("la_y", 2 * ny),
+        ("la", ny),
+        ("p_y", 2 * ny),
         ("x", 1),
         ("x_left", GROUPS),
         ("x_right", GROUPS),
@@ -122,17 +124,17 @@
         ("gx", pairs),
         ("gx_left", GROUPS),
         ("gx_right", GROUPS),
-        ("gbc", 1),
-        ("gbc_left", GROUPS),
-        ("gbc_right", GROUPS),
+        ("db_left", 1),
+        ("db_right", 1),
+        ("gx_g", 1),
+        ("cols", 1),
         ("ddt", 1),
         ("g_y", 2 * ny),
         ("g_core", 2),
         ("g_fwd", 2 * ny),
-        ("w1", 2),
         ("w2", 2 * chunks),
         ("w3", 2 * chunks),
-        ("w4", 2),
+        ("w4", 2 * chunks),
     )
     table = {}
     at = 0
@@ -176,6 +178,10 @@
     wball,
     wcall,
     cols,
+    lain,
+    psend,
+    pin,
+    psum,
     xin,
     dyin,
     dysend,
@@ -226,15 +232,13 @@
     colrow,
     dpx,
     gx,
-    dpbc,
-    gbc,
+    dbin,
     ddtsend,
     gsend,
+    ghid,
     gall,
     wsend,
     wown,
-    w1in,
-    s1send,
     w2in,
     s3send,
     ss,
@@ -263,7 +267,7 @@
     latent = wb_ref.shape[1]
     xc = heads * HEAD_DIM
     nsrc = sp // GROUPS
-    rows = cw // sp
+    rows = cw // chunks
     first = c == 0
     last = c == chunks - 1
     table, _ = slot_table(sp, dp, cores, pairs)
@@ -330,29 +334,39 @@
         )
     ):
         loads[at] = pltpu.make_async_copy(source, target, ls.at[at])
+    for at in (6, 2, 0, 1, 3, 4, 5):
         loads[at].start()
     greet(("dp", "sp"))
+    loads[6].wait()
+
+    phase("send_first")
+    cwy = cores * cw
+    part_rows = tokens // 2
+    parts = [slice(t * part_rows, (t + 1) * part_rows) for t in range(2)]
+    la_y = {}
+    for t in range(2):
+        for o in range(1, ny):
+            there = lax.rem(y + o, ny)
+            la_y[o, t] = go(
+                copy(
+                    la_ref.at[parts[t], lanes(there, cwy)],
+                    lain.at[y, parts[t], :],
+                    "la_y",
+                    2 * o + t,
+                    "dp",
+                    there * cores + core,
+                )
+            )
+    loads[2].wait()
+    x_copy = go(copy(x_ref.at[:, lanes(p, gw)], xin.at[mine, :], "x", 0, "sp", partner))
     loads[0].wait()
     loads[1].wait()
-
-    phase("send_first")
-    w_y = []
-    for o in range(1, ny):
-        peer = lax.rem(y + o, ny) * cores + core
-        w_y.append(
-            (
-                go(copy(wb_ref, wball.at[me_dp], "w_y", 2 * o, "dp", peer)),
-                go(copy(wc_ref, wcall.at[me_dp], "w_y", 2 * o + 1, "dp", peer)),
-            )
-        )
     w_core = []
     if cores > 1:
         w_core = [
             go(copy(wb_ref, wball.at[me_dp], "w_core", 0, "dp", other_core)),
             go(copy(wc_ref, wcall.at[me_dp], "w_core", 1, "dp", other_core)),
         ]
-    loads[2].wait()
-    x_copy = go(copy(x_ref.at[:, lanes(p, gw)], xin.at[mine, :], "x", 0, "sp", partner))
     dt_copy = go(
         copy(
             dt_ref.at[pl.ds(pl.multiple_of(p * gh, gh), gh), :],
@@ -457,20 +471,21 @@
     for o in range(1, sp):
         tap_copies.append(go(copy(tapsend, tapin.at[me_sp], "tap", o, "sp", lax.rem(me_sp + o, sp))))
     tapin[me_sp] = tapsend[...]
-    loads[6].wait()
     la_copies = []
-    for o in range(1, dp):
-        peer = lax.rem(me_dp + o, dp)
+    if cores > 1:
         la_copies.append(
-            go(copy(la_ref.at[:, lanes(peer, cw)], cols.at[me_dp], "la", o, "dp", peer))
+            go(copy(la_ref.at[:, lanes(other_core, cw)], cols.at[m, me_dp], "la", 0, "dp", other_core))
         )
-    cols[me_dp] = la_ref[:, lanes(me_dp, cw)]
+    cols[m, me_dp] = la_ref[:, lanes(me_dp, cw)]
+    wball[me_dp] = wb_ref[...]
+    wcall[me_dp] = wc_ref[...]
     xin[mine, :] = x_ref[:, lanes(m, gw)]
     dtin[:, lanes(m, tokens)] = dt_ref[pl.ds(pl.multiple_of(m * gh, gh), gh), :]
 
     phase("norm")
     width = inner // NORM_GROUPS
     per_half = NORM_GROUPS // GROUPS
+    early = per_half // 2
     dy_copies = []
     for at in (3, 4, 5):
         loads[at].wait()
@@ -492,12 +507,70 @@
             at = slice(i * width, (i + 1) * width)
             if half == 0:
                 dysend[:, at] = dy
-                dy_copies.append(
-                    go(copy(dysend.at[:, at], dyin.at[mine0, at], "dy", i, "sp", partner))
-                )
+                dy_copies.append(copy(dysend.at[:, at], dyin.at[mine0, at], "dy", i, "sp", partner))
+                if i < early:
+                    go(dy_copies[i])
             else:
                 dyin[mine0, at] = dy
 
+    phase("partial")
+    for item in w_core:
+        arrive(item)
+    p_y = {}
+    for t in range(2):
+        for o in range(1, ny):
+            there = lax.rem(y - o + ny, ny)
+            arrive(la_y[o, t])
+            tb = tc = None
+            for k in range(cores):
+                part = lain[there, parts[t], k * cw : (k + 1) * cw]
+                one, two = mm(part, wball[y * cores + k]), mm(part, wcall[y * cores + k])
+                tb, tc = (one, two) if tb is None else (tb + one, tc + two)
+            psend[there, parts[t], :latent] = tb.astype(bf16)
+            psend[there, parts[t], latent:] = tc.astype(bf16)
+            p_y[o, t] = go(
+                copy(
+                    psend.at[there, parts[t], :],
+                    pin.at[y, parts[t], :],
+                    "p_y",
+                    2 * o + t,
+                    "dp",
+                    there * cores + core,
+                )
+            )
+    w_y = []
+    for o in range(1, ny):
+        peer = lax.rem(y + o, ny) * cores + core
+        w_y.append(
+            (
+                go(copy(wb_ref, wball.at[me_dp], "w_y", 2 * o, "dp", peer)),
+                go(copy(wc_ref, wcall.at[me_dp], "w_y", 2 * o + 1, "dp", peer)),
+            )
+        )
+    for o in range(1, ny):
+        there = lax.rem(y - o + ny, ny)
+        block = there * cores + core
+        cols[m, block] = lain[there, :, lanes(core, cw)]
+        if cores > 1:
+            la_copies.append(
+                go(
+                    copy(
+                        lain.at[there, :, lanes(cores - 1 - core, cw)],
+                        cols.at[m, block],
+                        "la",
+                        o,
+                        "dp",
+                        other_core,
+                    )
+                )
+            )
+    total_b = total_c = None
+    for k in range(cores):
+        part = la_ref[:, lanes(y * cores + k, cw)]
+        one, two = mm(part, wball[y * cores + k]), mm(part, wcall[y * cores + k])
+        total_b, total_c = (one, two) if k == 0 else (total_b + one, total_c + two)
+    psum[:, :latent] = total_b
+    psum[:, latent:] = total_c
     phase("levels")
     arrive(dt_copy)
     for i in range(nsrc):
@@ -534,6 +607,23 @@
         tdec[j] = jnp.broadcast_to(jnp.exp2(-end), (8, LANES))
         dts_ref[j] = jnp.where(low_lane, dtcol[:, 2 * j : 2 * j + 1], dtcol[:, 2 * j + 1 : 2 * j + 2])
 
+    phase("project")
+    total = psum[...]
+    for o in range(1, ny):
+        for t in range(2):
+            arrive(p_y[o, t])
+        total = total + pin[lax.rem(y - o + ny, ny)].astype(f32)
+    total = total.astype(bf16)
+    proj_b, proj_c = total[:, :latent], total[:, latent:]
+    for g in range(GROUPS):
+        bcsend[g, :, :STATE] = proj_b[:, g * STATE : (g + 1) * STATE]
+        bcsend[g, :, STATE:] = proj_c[:, g * STATE : (g + 1) * STATE]
+    bc_copy = go(copy(bcsend.at[p], bcin.at[mine, :], "bc", 0, "sp", partner))
+    send_halo("bc", lambda g, r: bcsend.at[g, r, :], bcin)
+    bcin[mine, :] = bcsend[m]
+    for item in dy_copies[early:]:
+        go(item)
+
     phase("wait_x")
     for item in tap_copies:
         arrive(item)
@@ -562,52 +652,6 @@
         vb_ref[j] = v.astype(bf16)
         vef_ref[j] = (v * ef_ref[j]).astype(bf16)
         veb_ref[j] = (v * eb_ref[j]).astype(bf16)
-
-    phase("project")
-    wball[me_dp] = wb_ref[...]
-    wcall[me_dp] = wc_ref[...]
-
-    def project(total, index):
-        part = la_ref[:, lanes(index, cw)]
-        tb, tc = mm(part, wball[index]), mm(part, wcall[index])
-        return (tb, tc) if total is None else (total[0] + tb, total[1] + tc)
-
-    total = project(None, me_dp)
-    for item in w_core:
-        arrive(item)
-    if cores > 1:
-        total = project(total, other_core)
-    w_fwd = []
-    for o in range(1, ny):
-        src = lax.rem(y - o + ny, ny) * cores + core
-        for q in range(2):
-            arrive(w_y[o - 1][q])
-            if cores > 1:
-                full = (wball, wcall)[q].at[src]
-                w_fwd.append(go(copy(full, full, "w_fwd", 2 * o + q, "dp", other_core)))
-        total = project(total, src)
-    for o in range(1, ny):
-        if cores > 1:
-            arrive(w_fwd[2 * o - 2])
-            arrive(w_fwd[2 * o - 1])
-            total = project(total, lax.rem(y - o + ny, ny) * cores + cores - 1 - core)
-    proj_b, proj_c = total[0].astype(bf16), total[1].astype(bf16)
-    for g in range(GROUPS):
-        bcsend[g, :, :STATE] = proj_b[:, g * STATE : (g + 1) * STATE]
-        bcsend[g, :, STATE:] = proj_c[:, g * STATE : (g + 1) * STATE]
-    bc_copy = go(copy(bcsend.at[p], bcin.at[mine, :], "bc", 0, "sp", partner))
-    send_halo("bc", lambda g, r: bcsend.at[g, r, :], bcin)
-    bcin[mine, :] = bcsend[m]
-
-    phase("wait_dy")
-    for item in dy_copies:
-        arrive(item)
-
-    @pl.loop(0, pairs)
-    def _(j):
-        dy = dyin[:, lanes(j, LANES)].astype(f32)
-        dyef_ref[j] = (dy * ef_ref[j]).astype(bf16)
-        dyeb_ref[j] = (dy * eb_ref[j]).astype(bf16)
 
     phase("wait_bc")
     arrive(bc_copy)
@@ -738,11 +782,24 @@
 
     delay = SKEW * (chunks - 1)
 
+    for item in la_copies:
+        arrive(item)
+    cols_copy = go(copy(cols.at[m], cols.at[m], "cols", 0, "sp", partner))
     phase("ticks")
     @pl.loop(0, pairs + delay)
     def _(tick):
+        per = width // LANES
+
+        @pl.when(jnp.logical_and(tick < pairs, lax.rem(tick, per) == 0))
+        def _():
+            piece = lanes(tick // per, width)
+            arrive(copy(dysend.at[:, piece], dyin.at[mine0, piece], "dy", tick // per, "sp", partner))
+
         @pl.when(tick < pairs)
         def _():
+            dy = dyin[:, lanes(tick, LANES)].astype(f32)
+            dyef_ref[tick] = (dy * ef_ref[tick]).astype(bf16)
+            dyeb_ref[tick] = (dy * eb_ref[tick]).astype(bf16)
             sr_ref[tick, 0] = mm(kt[...], veb_ref[tick])
             sr_ref[tick, 1] = mm(rt[...], dyeb_ref[tick])
             sl_ref[tick, 0] = mm(kt[...], vef_ref[tick])
@@ -780,17 +837,19 @@
 
     phase("send_dbc")
     sbc = sbc_ref[...]
-    dpbc[:, :STATE] = (dksum[...] * sbc[:, :STATE]).astype(bf16)
-    dpbc[:, STATE:] = (drsum[...] * sbc[:, STATE:]).astype(bf16)
-    gbc_copy = go(
+    dbin[body, :STATE] = (dksum[...] * sbc[:, :STATE]).astype(bf16)
+    dbin[body, STATE:] = (drsum[...] * sbc[:, STATE:]).astype(bf16)
+    go(
         copy(
-            dpbc.at[pl.ds(pl.multiple_of(p * (tokens - HALO), HALO), tokens + HALO), :],
-            gbc.at[m, pl.ds(pl.multiple_of(HALO - HALO * p, HALO), tokens + HALO), :],
-            "gbc",
-            0,
-            "sp",
-            partner,
-        )
+            dbin.at[ch : HALO + ch, :], dbin.at[left_rows, :], "db_left", 0, "sp", near(GROUPS)
+        ),
+        jnp.logical_not(last),
+    )
+    go(
+        copy(
+            dbin.at[HALO : 2 * HALO, :], dbin.at[right_rows, :], "db_right", 0, "sp", near(-GROUPS)
+        ),
+        jnp.logical_not(first),
     )
 
     def send_edges(name, source, target):
@@ -841,12 +900,19 @@
         def _():
             target[:, HALO + tokens :, :] = jnp.zeros((GROUPS, HALO, target.shape[2]), bf16)
 
-    send_edges("gbc", dpbc, gbc)
     gx_copy(pairs - 1).start()
     send_edges("gx", dpx, gx)
-    gbc[m, keep_dst, :] = dpbc[keep_src, :]
 
     phase("ddt")
+    w_fwd = []
+    for o in range(1, ny):
+        src = lax.rem(y - o + ny, ny) * cores + core
+        for q in range(2):
+            arrive(w_y[o - 1][q])
+            if cores > 1:
+                full = (wball, wcall)[q].at[src]
+                w_fwd.append(go(copy(full, full, "w_fwd", 2 * o + q, "dp", other_core)))
+
     fill = jnp.zeros((LANES - gh, ch), f32)
     down = jnp.concatenate([colrow[...], fill], axis=0).T
     drate = jnp.dot(upper, dlev[...] - down, precision=highest, preferred_element_type=f32)
@@ -858,20 +924,16 @@
     ddt_copy = go(copy(ddtsend.at[p], ddt_ref.at[group_rows, :], "ddt", 0, "sp", partner))
     ddt_ref[group_rows, :] = ddtsend[m]
 
-    phase("wait_gbc")
-    arrive(gbc_copy)
-    await_edges("gbc", gbc)
+    phase("wait_db")
+    await_halo("db", dbin)
     phase("conv_g")
-    for g in range(GROUPS):
-        for q in range(2):
-            at = slice(g * STATE, (g + 1) * STATE)
-            taps = (tapb_ref, tapc_ref)[q][:, at]
-            part = gbc[g, :, q * STATE : (q + 1) * STATE].astype(f32)
-            to = q * latent + g * STATE
-            gsend[:, to : to + STATE] = window_conv(part, taps, tokens, True).astype(bf16)
-
-    phase("d_hidden")
-    halves = [slice(q * latent, (q + 1) * latent) for q in range(2)]
+    for q in range(2):
+        at = slice(q * STATE, (q + 1) * STATE)
+        taps = (tapb_ref, tapc_ref)[q][:, lanes(m, STATE)]
+        gsend[:, at] = window_conv(dbin[:, at].astype(f32), taps, ch, True).astype(bf16)
+
+    phase("send_g")
+    halves = [slice(q * STATE, (q + 1) * STATE) for q in range(2)]
 
     def g_copy(source, block, name, index, q, peer):
         return go(
@@ -893,14 +955,12 @@
             g_y[o, q] = g_copy(gsend, me_dp, "g_y", o, q, peer)
         if cores > 1:
             g_core[q] = g_copy(gsend, me_dp, "g_core", 0, q, other_core)
+    theirs = pl.ds(pl.multiple_of(p * tokens, HALO), tokens)
+    hid_copy = go(copy(gsend.at[theirs, :], ghid.at[m], "gx_g", 0, "sp", partner))
+    ghid[m] = gsend[mine0, :]
     gall[me_dp] = gsend[...]
-    gb, gc = gsend[:, :latent], gsend[:, latent:]
-    for i in range(dp):
-        dh_ref[:, i * cw : (i + 1) * cw] = (mm_nt(gb, wball[i]) + mm_nt(gc, wcall[i])).astype(bf16)
     phase("wait_g")
-    for item in la_copies:
-        arrive(item)
-    w1 = []
+    arrive(cols_copy)
     g_fwd = {}
 
     def forward_g(q):
@@ -910,6 +970,7 @@
             if cores > 1:
                 g_fwd[o, q] = g_copy(gall.at[src], src, "g_fwd", o, q, other_core)
 
+    w2 = {}
     forward_g(0)
     for q in range(2):
         if cores > 1:
@@ -920,12 +981,28 @@
             forward_g(1)
         phase("dw")
         total = None
-        for i in range(dp):
-            term = mm_tn(cols[i], gall[i, :, halves[q]])
-            total = term if total is None else total + term
-        total = total.reshape(GROUPS, chunks, rows, latent)
-        wsend[q] = total.astype(bf16)
-        w1.append(go(copy(wsend.at[q, p], w1in.at[q], "w1", q, "sp", partner)))
+        for g in range(GROUPS):
+            for i in range(dp):
+                term = mm_tn(gall[i, g * tokens : (g + 1) * tokens, halves[q]], cols[g, i])
+                total = term if total is None else total + term
+        wown[q] = total.T.reshape(chunks, rows, STATE)
+        wsend[q] = wown[q].astype(bf16)
+        for o in range(1, chunks):
+            k = lax.rem(c + o, chunks)
+            w2[q, o] = go(
+                copy(
+                    wsend.at[q, k], w2in.at[q, c], "w2", q * chunks + o, "sp", k * GROUPS + m
+                )
+            )
+
+    phase("d_hidden")
+    for item in w_fwd:
+        arrive(item)
+    arrive(hid_copy)
+    gb = jnp.concatenate([ghid[g, :, :STATE] for g in range(GROUPS)], axis=1)
+    gc = jnp.concatenate([ghid[g, :, STATE:] for g in range(GROUPS)], axis=1)
+    for i in range(dp):
+        dh_ref[:, i * cw : (i + 1) * cw] = (mm_nt(gb, wball[i]) + mm_nt(gc, wcall[i])).astype(bf16)
 
     def input_gradient(g):
         @pl.loop(0, pairs)
@@ -942,60 +1019,32 @@
         gx_copy(j).wait_recv()
 
     await_edges("gx", gx)
-    phase("w2")
-    w2 = []
+    phase("w3")
+    w3 = {}
+    w4 = []
     for q in range(2):
-        arrive(w1[q])
-        part = wsend[q, m].astype(f32) + w1in[q].astype(f32)
-        s1send[q] = part.astype(bf16)
+        share = wown[q, c]
         for o in range(1, chunks):
-            k = lax.rem(c + o, chunks)
-            w2.append(
-                go(
-                    copy(
-                        s1send.at[q, k],
-                        w2in.at[q, c],
-                        "w2",
-                        q * chunks + o,
-                        "sp",
-                        k * GROUPS + m,
-                    )
-                )
-            )
-        wown[q] = s1send[q, c].astype(f32)
-    phase("dx0")
-    input_gradient(0)
-    phase("w3")
-    w3 = []
-    for q in range(2):
-        share = wown[q]
-        for o in range(1, chunks):
-            arrive(w2[q * (chunks - 1) + o - 1])
+            arrive(w2[q, o])
             share = share + w2in[q, lax.rem(c - o + chunks, chunks)].astype(f32)
         s3send[q] = share.astype(bf16)
         tall[q, m, c] = s3send[q]
         for o in range(1, chunks):
             k = lax.rem(c + o, chunks)
-            w3.append(
-                go(
-                    copy(
-                        s3send.at[q],
-                        tall.at[q, m, c],
-                        "w3",
-                        q * chunks + o,
-                        "sp",
-                        k * GROUPS + m,
-                    )
+            w3[q, o] = go(
+                copy(
+                    s3send.at[q], tall.at[q, m, c], "w3", q * chunks + o, "sp", k * GROUPS + m
                 )
             )
-    phase("dx1")
-    input_gradient(1)
+        w4.append(go(copy(s3send.at[q], tall.at[q, m, c], "w4", q * chunks, "sp", partner)))
+        phase("dx")
+        input_gradient(q)
     phase("w4")
-    w4 = []
     for q in range(2):
         for o in range(1, chunks):
-            arrive(w3[q * (chunks - 1) + o - 1])
-        w4.append(go(copy(tall.at[q, m], tall.at[q, m], "w4", q, "sp", partner)))
+            arrive(w3[q, o])
+            piece = tall.at[q, m, lax.rem(c - o + chunks, chunks)]
+            w4.append(go(copy(piece, piece, "w4", q * chunks + o, "sp", partner)))
     phase("last")
     arrive(ddt_copy)
     for item in w4:
@@ -1027,13 +1076,31 @@
     phase.end()
 
 
-def out_kernel(dgate, dx, dh, ddt, tall, dgate_out, dx_out, dh_out, ddt_out, dwb_out, dwc_out):
-    ddt_out[...] = ddt[...]
-    dgate_out[...] = dgate[...]
-    dx_out[...] = dx[...]
-    dh_out[...] = dh[...]
-    dwb_out[...] = tall[0].astype(f32).reshape(dwb_out.shape)
-    dwc_out[...] = tall[1].astype(f32).reshape(dwc_out.shape)
+def out_kernel(
+    dgate, dx, dh, ddt, tall, dgate_out, dx_out, dh_out, ddt_out, dwb_out, dwc_out, wide, sems
+):
+    copies = [
+        pltpu.make_async_copy(source, target, sems.at[at])
+        for at, (source, target) in enumerate(
+            (
+                (dgate, dgate_out),
+                (dx, dx_out),
+                (dh, dh_out),
+                (ddt, ddt_out),
+                (wide.at[0], dwb_out),
+                (wide.at[1], dwc_out),
+            )
+        )
+    ]
+    for item in copies[:4]:
+        item.start()
+    for q in range(2):
+        for g in range(GROUPS):
+            at = slice(g * STATE, (g + 1) * STATE)
+            wide[q, :, at] = tall[q, g].astype(f32).reshape(wide.shape[1], STATE)
+        copies[4 + q].start()
+    for item in copies:
+        item.wait()
 
 
 def local(
@@ -1069,7 +1136,7 @@
     gw = inner // GROUPS
     gh = HEADS // GROUPS
     pairs = gw // LANES
-    rows = cw // sp
+    rows = cw // chunks
     window = tokens * sp
     _, slots = slot_table(sp, dp, cores, pairs)
 
@@ -1086,7 +1153,11 @@
         ((tokens, inner), bf16),
         ((dp, cw, latent), bf16),
         ((dp, cw, latent), bf16),
-        ((dp, tokens, cw), bf16),
+        ((GROUPS, dp, tokens, cw), bf16),
+        ((dp // cores, tokens, cores * cw), bf16),
+        ((dp // cores, tokens, 2 * latent), bf16),
+        ((dp // cores, tokens, 2 * latent), bf16),
+        ((tokens, 2 * latent), f32),
         ((ch + 2 * HALO, gw), bf16),
         ((ch, gw), bf16),
         ((tokens, gw), bf16),
@@ -1137,17 +1208,15 @@
         ((gh, ch), f32),
         ((ch, gw), bf16),
         ((GROUPS, tokens + 2 * HALO, gw), bf16),
+        ((ch + 2 * HALO, 2 * STATE), bf16),
+        ((GROUPS, gh, tokens), bf16),
         ((ch, 2 * STATE), bf16),
-        ((GROUPS, tokens + 2 * HALO, 2 * STATE), bf16),
-        ((GROUPS, gh, tokens), bf16),
-        ((tokens, 2 * latent), bf16),
-        ((dp, tokens, 2 * latent), bf16),
-        ((2, GROUPS, chunks, rows, latent), bf16),
-        ((2, rows, latent), f32),
-        ((2, chunks, rows, latent), bf16),
-        ((2, chunks, rows, latent), bf16),
-        ((2, chunks, rows, latent), bf16),
-        ((2, rows, latent), bf16),
+        ((GROUPS, tokens, 2 * STATE), bf16),
+        ((dp, ch, 2 * STATE), bf16),
+        ((2, chunks, rows, STATE), bf16),
+        ((2, chunks, rows, STATE), f32),
+        ((2, chunks, rows, STATE), bf16),
+        ((2, rows, STATE), bf16),
     ]
     dgate, dx, ddt, dh, tall = pl.pallas_call(
         functools.partial(mega_kernel, heads, cores),
@@ -1158,7 +1227,7 @@
             pltpu.VMEM((tokens, inner), bf16),
             pltpu.VMEM((HEADS, tokens), bf16),
             pltpu.VMEM((tokens, width_in), bf16),
-            pltpu.VMEM((2, GROUPS, chunks, rows, latent), bf16),
+            pltpu.VMEM((2, GROUPS, chunks, rows, STATE), bf16),
         ],
         scratch_shapes=[pltpu.VMEM(shape, kind) for shape, kind in scratch]
         + [pltpu.SemaphoreType.DMA((slots,)), pltpu.SemaphoreType.DMA((slots,))]
@@ -1188,7 +1257,8 @@
     d_gate, d_x, d_hidden, d_dt, d_w_b, d_w_c = pl.pallas_call(
         out_kernel,
         in_specs=[vmem] * 5,
-        out_specs=[vmem] * 6,
+        out_specs=[hbm] * 6,
+        scratch_shapes=[pltpu.VMEM((2, cw, latent), f32), pltpu.SemaphoreType.DMA((6,))],
         out_shape=[
             jax.ShapeDtypeStruct((tokens, inner), bf16),
             jax.ShapeDtypeStruct((tokens, inner), bf16),

time: 83.5 us -> 75.2 us (0.901)
  Pallas kernels: 82.7 us -> 74.3 us
    pallas_call x1, Pallas kernels: 81 us -> 72.7 us  [local(): pl.pallas_call(functools.partial(mega_kernel, heads, cores), in_specs=[hb...]
where the time goes in v3:
time: 75.2 us; the launch traced here: 74.9 us
  Pallas kernels  74.3 us (99%)
    pallas_call x1, Pallas kernels, local(): pl.pallas_call(functools.partial(mega_kernel, heads, cores), in_specs=[hb...  72.7 us
    pallas_call x1, Pallas kernels, local(): pl.pallas_call(out_kernel, in_specs=[vmem] * 5, out_specs=[hbm] * 6, scra...  1.54 us

profile of v3, /device:TPU:0, one launch (start us, length us, event | category | flops | bytes accessed | tf_op | source)
XLA Modules:
  0.0 74.9 jit_solution(5201923155792845295)
XLA Ops:
  0.6 72.7 %mega.1 = (bf16[128,2048]{1,0:T(8,128)(2,1)S(1)}, bf16[128,2048]{1,0:T(8,128)(2,1)S(1)}, bf16[32,128]{1,0:T(8,128)(2,1)S(1)}, bf16[128,2048]{1,0:T(8,128)(2,1)S(1)}, bf16[2,2,4,128,128]{4,3,2,1,0:T(8,128)(2,1)S(1)}) custom-call(bf16[128,2048]{1,0:T(8,128)(2,1)} %bitcast.18, bf16[512,256]{1,0:T(8,128)(2,1)} %wb_hbm.1, bf16[512,256]{1,0:T(8,128)(2,1)} %wc_hbm.1, ...), custom_call_target="tpu_custom_call" | custom-call | tf_op jit(solution)/shard_map/mega/pallas_call | solution.py:1221
  73.4 1.5 %outputs.1 = (bf16[128,2048]{1,0:T(8,128)(2,1)}, bf16[128,2048]{1,0:T(8,128)(2,1)}, bf16[128,2048]{1,0:T(8,128)(2,1)}, bf16[32,128]{1,0:T(8,128)(2,1)}, f32[512,256]{1,0:T(8,128)}, /*index=5*/f32[512,256]{1,0:T(8,128)}) custom-call(bf16[128,2048]{1,0:T(8,128)(2,1)S(1)} %get-tuple-element.17.dgate, bf16[128,2048]{1,0:T(8,128)(2,1)S(1)} %get-tuple-element.18.dx, ...), custom_call_target="tpu_custom_call" | custom-call | tf_op jit(solution)/shard_map/outputs/pallas_call | solution.py:1257

commit v4 on v3

--- a/solution.py
+++ b/solution.py
@@ -15,7 +15,8 @@
 CONV_K = 5
 LANES = 128
 HALO = 16
-SKEW = 2
+SKEW = 3
+PIECES = 4
 EPSILON = 1e-06
 LOG2E = 1.4426950408889634
 highest = lax.Precision.HIGHEST
@@ -99,49 +100,51 @@
             self.scope = None
 
 
-def slot_table(sp, dp, cores, pairs):
-    ny = dp // cores
+def slot_tables(sp, dp, cores, pairs):
+    others = dp // cores - 1
     chunks = sp // GROUPS
+    away = max(chunks - 1, 1)
     counts = (
-        ("w_y", 2 * ny),
-        ("w_core", 2),
-        ("w_fwd", 2 * ny),
-        ("la_y", 2 * ny),
-        ("la", ny),
-        ("p_y", 2 * ny),
-        ("x", 1),
-        ("x_left", GROUPS),
-        ("x_right", GROUPS),
-        ("dt", 1),
-        ("drop", chunks),
-        ("tap", sp),
-        ("dy", NORM_GROUPS),
-        ("bc", 1),
-        ("bc_left", GROUPS),
-        ("bc_right", GROUPS),
-        ("right", 2 * pairs),
-        ("left", 2 * pairs),
-        ("gx", pairs),
-        ("gx_left", GROUPS),
-        ("gx_right", GROUPS),
-        ("db_left", 1),
-        ("db_right", 1),
-        ("gx_g", 1),
-        ("cols", 1),
-        ("ddt", 1),
-        ("g_y", 2 * ny),
-        ("g_core", 2),
-        ("g_fwd", 2 * ny),
-        ("w2", 2 * chunks),
-        ("w3", 2 * chunks),
-        ("w4", 2 * chunks),
+        ("w_y", 2 * others, 2 * others),
+        ("w_core", 2, 2),
+        ("w_fwd", 2 * others, 2 * others),
+        ("la_y", PIECES * others, PIECES * others),
+        ("la", others + 1, others + 1),
+        ("p_y", PIECES * others, PIECES * others),
+        ("x", 1, 1),
+        ("x_left", 1, 1),
+        ("x_right", 1, 1),
+        ("dt", 1, 1),
+        ("drop", 2, 1),
+        ("tap", 1, 1),
+        ("dy", 1, NORM_GROUPS // GROUPS),
+        ("bc", PIECES, PIECES),
+        ("bc_left", 1, 1),
+        ("bc_right", 1, 1),
+        ("right", 4, 2 * pairs),
+        ("left", 4, 2 * pairs),
+        ("gx", 1, 1),
+        ("gx_left", 1, GROUPS),
+        ("gx_right", 1, GROUPS),
+        ("db_left", 1, 1),
+        ("db_right", 1, 1),
+        ("gx_g", 1, 1),
+        ("cols", 1, 1),
+        ("ddt", 1, 1),
+        ("g_y", 2 * others, 2 * others),
+        ("g_core", 2, 2),
+        ("g_fwd", 2 * others, 2 * others),
+        ("w2", 2, 2),
+        ("w3", 2, 2 * away),
+        ("w4", 1, 1),
     )
-    table = {}
-    at = 0
-    for name, count in counts:
-        table[name] = at
-        at += count
-    return table, at
+    sends, arrivals = {}, {}
+    send_at = arrive_at = 0
+    for name, send_count, arrive_count in counts:
+        sends[name], arrivals[name] = send_at, arrive_at
+        send_at += send_count
+        arrive_at += arrive_count
+    return sends, arrivals, max(send_at, 1), max(arrive_at, 1)
 
 
 def mega_kernel(
@@ -237,6 +240,7 @@
     gsend,
     ghid,
     gall,
+    wtot,
     wsend,
     wown,
     w2in,
@@ -270,21 +274,20 @@
     rows = cw // chunks
     first = c == 0
     last = c == chunks - 1
-    table, _ = slot_table(sp, dp, cores, pairs)
+    sends, arrivals, _, _ = slot_tables(sp, dp, cores, pairs)
     sent = []
 
     def copy(src, dst, name, index, axis, peer, into=None):
-        at = table[name]
         return pltpu.make_async_remote_copy(
             src_ref=src,
             dst_ref=dst,
-            send_sem=ss.at[at + index],
-            recv_sem=rs.at[at + (index if into is None else into)],
+            send_sem=ss.at[sends[name] + index],
+            recv_sem=rs.at[arrivals[name] + (index if into is None else into)],
             device_id={axis: peer},
             device_id_type=pl.DeviceIdType.MESH,
         )
 
-    def go(item, cond=None):
+    def go(item, cond=None, alone=True):
         if cond is None:
             item.start()
         else:
@@ -293,8 +296,12 @@
             def _():
                 item.start()
 
-        sent.append((item, cond))
+        if alone:
+            sent.append((item, cond))
         return item
+
+    def together(name, index, region, cond=None):
+        sent.append((copy(region, region, name, index, "sp", partner), cond))
 
     def arrive(item, cond=None):
         if cond is None:
@@ -341,10 +348,10 @@
 
     phase("send_first")
     cwy = cores * cw
-    part_rows = tokens // 2
-    parts = [slice(t * part_rows, (t + 1) * part_rows) for t in range(2)]
+    part_rows = tokens // PIECES
+    parts = [slice(t * part_rows, (t + 1) * part_rows) for t in range(PIECES)]
     la_y = {}
-    for t in range(2):
+    for t in range(PIECES):
         for o in range(1, ny):
             there = lax.rem(y + o, ny)
             la_y[o, t] = go(
@@ -352,7 +359,7 @@
                     la_ref.at[parts[t], lanes(there, cwy)],
                     lain.at[y, parts[t], :],
                     "la_y",
-                    2 * o + t,
+                    PIECES * (o - 1) + t,
                     "dp",
                     there * cores + core,
                 )
@@ -385,25 +392,29 @@
                     source(g, slice(tokens - HALO, tokens)),
                     target.at[left_rows, :],
                     name + "_left",
-                    g,
+                    0,
                     "sp",
                     near(1 + g),
                     into=0,
                 ),
                 to_right,
+                alone=False,
             )
             go(
                 copy(
                     source(g, slice(0, HALO)),
                     target.at[right_rows, :],
                     name + "_right",
-                    g,
+                    0,
                     "sp",
                     near(g - GROUPS),
                     into=0,
                 ),
                 to_left,
-            )
+                alone=False,
+            )
+        together(name + "_left", 0, target.at[: GROUPS * HALO, :], to_right)
+        together(name + "_right", 0, target.at[: GROUPS * HALO, :], to_left)
 
     def await_halo(name, target):
         arrive(
@@ -447,13 +458,16 @@
                 dropsend.at[k],
                 dropin.at[place],
                 "drop",
-                o,
+                0 if o else 1,
                 "sp",
                 k * GROUPS + owner if o else partner,
-                into=place,
+                into=0,
             ),
             None if o else owner != m,
-        )
+            alone=not o,
+        )
+    if chunks > 1:
+        together("drop", 0, dropsend.at[: chunks - 1])
 
     @pl.when(owner == m)
     def _():
@@ -467,9 +481,10 @@
     tapsend[...] = jnp.zeros_like(tapsend)
     tapsend[:CONV_K, :xc] = tapx_ref[...]
     tapsend[CONV_K : CONV_K + 1, :] = skips
-    tap_copies = []
     for o in range(1, sp):
-        tap_copies.append(go(copy(tapsend, tapin.at[me_sp], "tap", o, "sp", lax.rem(me_sp + o, sp))))
+        go(copy(tapsend, tapin.at[me_sp], "tap", 0, "sp", lax.rem(me_sp + o, sp)), alone=False)
+    all_taps = tapin.at[: sp - 1]
+    together("tap", 0, all_taps)
     tapin[me_sp] = tapsend[...]
     la_copies = []
     if cores > 1:
@@ -507,9 +522,11 @@
             at = slice(i * width, (i + 1) * width)
             if half == 0:
                 dysend[:, at] = dy
-                dy_copies.append(copy(dysend.at[:, at], dyin.at[mine0, at], "dy", i, "sp", partner))
+                dy_copies.append(
+                    copy(dysend.at[:, at], dyin.at[mine0, at], "dy", 0, "sp", partner, into=i)
+                )
                 if i < early:
-                    go(dy_copies[i])
+                    go(dy_copies[i], alone=False)
             else:
                 dyin[mine0, at] = dy
 
@@ -517,7 +534,7 @@
     for item in w_core:
         arrive(item)
     p_y = {}
-    for t in range(2):
+    for t in range(PIECES):
         for o in range(1, ny):
             there = lax.rem(y - o + ny, ny)
             arrive(la_y[o, t])
@@ -533,7 +550,7 @@
                     psend.at[there, parts[t], :],
                     pin.at[y, parts[t], :],
                     "p_y",
-                    2 * o + t,
+                    PIECES * (o - 1) + t,
                     "dp",
                     there * cores + core,
                 )
@@ -543,8 +560,8 @@
         peer = lax.rem(y + o, ny) * cores + core
         w_y.append(
             (
-                go(copy(wb_ref, wball.at[me_dp], "w_y", 2 * o, "dp", peer)),
-                go(copy(wc_ref, wcall.at[me_dp], "w_y", 2 * o + 1, "dp", peer)),
+                go(copy(wb_ref, wball.at[me_dp], "w_y", 2 * o - 2, "dp", peer)),
+                go(copy(wc_ref, wcall.at[me_dp], "w_y", 2 * o - 1, "dp", peer)),
             )
         )
     for o in range(1, ny):
@@ -573,10 +590,11 @@
     psum[:, latent:] = total_c
     phase("levels")
     arrive(dt_copy)
+    if nsrc > 1:
+        some = dropin.at[: nsrc - 1]
+        arrive(copy(some, some, "drop", 0, "sp", partner), owner == m)
+    arrive(copy(dropin, dropin, "drop", 0, "sp", partner), owner != m)
     for i in range(nsrc):
-        arrive(
-            copy(dropsend.at[0], dropin.at[i], "drop", i, "sp", partner), m * nsrc + i != me_sp
-        )
         drow[i * heads : (i + 1) * heads, :] = dropin[i, :heads, :]
     twice = lambda v: jnp.concatenate([v] * (ch // LANES), axis=1)
     fade = jnp.exp(drow[:, ch + LANES :])
@@ -608,25 +626,30 @@
         dts_ref[j] = jnp.where(low_lane, dtcol[:, 2 * j : 2 * j + 1], dtcol[:, 2 * j + 1 : 2 * j + 2])
 
     phase("project")
-    total = psum[...]
-    for o in range(1, ny):
-        for t in range(2):
+    bc_copies = []
+    for t in range(PIECES):
+        total = psum[parts[t], :]
+        for o in range(1, ny):
             arrive(p_y[o, t])
-        total = total + pin[lax.rem(y - o + ny, ny)].astype(f32)
-    total = total.astype(bf16)
-    proj_b, proj_c = total[:, :latent], total[:, latent:]
-    for g in range(GROUPS):
-        bcsend[g, :, :STATE] = proj_b[:, g * STATE : (g + 1) * STATE]
-        bcsend[g, :, STATE:] = proj_c[:, g * STATE : (g + 1) * STATE]
-    bc_copy = go(copy(bcsend.at[p], bcin.at[mine, :], "bc", 0, "sp", partner))
+            total = total + pin[lax.rem(y - o + ny, ny), parts[t], :].astype(f32)
+        total = total.astype(bf16)
+        for g in range(GROUPS):
+            at = slice(g * STATE, (g + 1) * STATE)
+            bcsend[g, parts[t], :STATE] = total[:, at]
+            at = slice(latent + g * STATE, latent + (g + 1) * STATE)
+            bcsend[g, parts[t], STATE:] = total[:, at]
+        into = pl.ds(pl.multiple_of(HALO + m * tokens + t * part_rows, HALO), part_rows)
+        bc_copies.append(
+            go(copy(bcsend.at[p, parts[t], :], bcin.at[into, :], "bc", t, "sp", partner))
+        )
     send_halo("bc", lambda g, r: bcsend.at[g, r, :], bcin)
     bcin[mine, :] = bcsend[m]
     for item in dy_copies[early:]:
-        go(item)
+        go(item, alone=False)
+    together("dy", 0, dysend)
 
     phase("wait_x")
-    for item in tap_copies:
-        arrive(item)
+    arrive(copy(all_taps, all_taps, "tap", 0, "sp", partner))
     if xc % LANES == 0:
         for i in range(sp):
             tapall[:, i * xc : (i + 1) * xc] = tapin[i]
@@ -654,7 +677,8 @@
         veb_ref[j] = (v * eb_ref[j]).astype(bf16)
 
     phase("wait_bc")
-    arrive(bc_copy)
+    for item in bc_copies:
+        arrive(item)
     await_halo("bc", bcin)
     phase("conv_bc")
     for q in range(2):
@@ -726,7 +750,7 @@
                 m, pl.ds(pl.multiple_of(HALO - HALO * p, HALO), tokens + HALO), lanes(j, LANES)
             ],
             "gx",
-            j,
+            0,
             "sp",
             partner,
         )
@@ -763,7 +787,15 @@
         cross[...] += split_mm(over, onehot)
 
     def chain_copy(name, j, q, into_ref, out_ref, step):
-        return copy(out_ref.at[j, q], into_ref.at[j, q], name, 2 * j + q, "sp", near(step))
+        return copy(
+            out_ref.at[j, q],
+            into_ref.at[j, q],
+            name,
+            2 * lax.rem(j, 2) + q,
+            "sp",
+            near(step),
+            into=2 * j + q,
+        )
 
     def chain(name, j, into_ref, own_ref, out_ref, head, tail, step):
         decay = tdec[j][0:1, :]
@@ -778,6 +810,10 @@
 
             @pl.when(jnp.logical_not(tail))
             def _():
+                @pl.when(j >= 2)
+                def _():
+                    chain_copy(name, j - 2, q, into_ref, out_ref, step).wait_send()
+
                 item.start()
 
     delay = SKEW * (chunks - 1)
@@ -793,7 +829,8 @@
         @pl.when(jnp.logical_and(tick < pairs, lax.rem(tick, per) == 0))
         def _():
             piece = lanes(tick // per, width)
-            arrive(copy(dysend.at[:, piece], dyin.at[mine0, piece], "dy", tick // per, "sp", partner))
+            block = dyin.at[mine0, piece]
+            arrive(copy(block, block, "dy", 0, "sp", partner, into=tick // per))
 
         @pl.when(tick < pairs)
         def _():
@@ -883,12 +920,12 @@
         for g in range(GROUPS):
             slot = target.at[g, :HALO, :]
             arrive(
-                copy(slot, slot, name + "_left", g, "sp", partner),
+                copy(slot, slot, name + "_left", 0, "sp", partner, into=g),
                 jnp.logical_and(lead, jnp.logical_not(first)),
             )
             slot = target.at[g, HALO + tokens :, :]
             arrive(
-                copy(slot, slot, name + "_right", g, "sp", partner),
+                copy(slot, slot, name + "_right", 0, "sp", partner, into=g),
                 jnp.logical_and(trail, jnp.logical_not(last)),
             )
 
@@ -911,7 +948,7 @@
             arrive(w_y[o - 1][q])
             if cores > 1:
                 full = (wball, wcall)[q].at[src]
-                w_fwd.append(go(copy(full, full, "w_fwd", 2 * o + q, "dp", other_core)))
+                w_fwd.append(go(copy(full, full, "w_fwd", 2 * o - 2 + q, "dp", other_core)))
 
     fill = jnp.zeros((LANES - gh, ch), f32)
     down = jnp.concatenate([colrow[...], fill], axis=0).T
@@ -952,7 +989,7 @@
     for q in range(2):
         for o in range(1, ny):
             peer = lax.rem(y + o, ny) * cores + core
-            g_y[o, q] = g_copy(gsend, me_dp, "g_y", o, q, peer)
+            g_y[o, q] = g_copy(gsend, me_dp, "g_y", o - 1, q, peer)
         if cores > 1:
             g_core[q] = g_copy(gsend, me_dp, "g_core", 0, q, other_core)
     theirs = pl.ds(pl.multiple_of(p * tokens, HALO), tokens)
@@ -961,39 +998,73 @@
     gall[me_dp] = gsend[...]
     phase("wait_g")
     arrive(cols_copy)
+    sources = {o: lax.rem(y - o + ny, ny) * cores + core for o in range(1, ny)}
+    relayed = {o: lax.rem(y - o + ny, ny) * cores + cores - 1 - core for o in range(1, ny)}
     g_fwd = {}
-
-    def forward_g(q):
+    w2 = {}
+    for q in range(2):
         for o in range(1, ny):
-            src = lax.rem(y - o + ny, ny) * cores + core
+            if cores > 1:
+                block = gall.at[sources[o], :, halves[q]]
+                g_fwd[o, q] = copy(
+                    block, block, "g_fwd", 2 * (o - 1) + q, "dp", other_core
+                )
+                sent.append((g_fwd[o, q], None))
+        for o in range(1, chunks):
+            k = lax.rem(c + o, chunks)
+            w2[q, o] = copy(
+                wsend.at[q, k], w2in.at[q, c], "w2", q, "sp", k * GROUPS + m
+            )
+        if chunks > 1:
+            together("w2", q, w2in.at[q, : chunks - 1])
+
+    def add_block(q, i, fresh=False):
+        total = None
+        for g in range(GROUPS):
+            term = mm_tn(gall[i, g * tokens : (g + 1) * tokens, halves[q]], cols[g, i])
+            total = term if total is None else total + term
+        wtot[q] = total if fresh else wtot[q] + total
+
+    def add_peers(q):
+        for o in range(1, ny):
             arrive(g_y[o, q])
             if cores > 1:
-                g_fwd[o, q] = g_copy(gall.at[src], src, "g_fwd", o, q, other_core)
-
-    w2 = {}
-    forward_g(0)
-    for q in range(2):
+                g_fwd[o, q].start()
+            add_block(q, sources[o])
+
+    def add_other_core(q):
         if cores > 1:
             arrive(g_core[q])
+            add_block(q, other_core)
             for o in range(1, ny):
                 arrive(g_fwd[o, q])
-        if q == 0:
-            forward_g(1)
-        phase("dw")
-        total = None
-        for g in range(GROUPS):
-            for i in range(dp):
-                term = mm_tn(gall[i, g * tokens : (g + 1) * tokens, halves[q]], cols[g, i])
-                total = term if total is None else total + term
-        wown[q] = total.T.reshape(chunks, rows, STATE)
-        wsend[q] = wown[q].astype(bf16)
+                add_block(q, relayed[o])
+
+    def scatter(q):
+        total = wtot[q].T.reshape(chunks, rows, STATE)
+        wown[q] = total
+        wsend[q] = total.astype(bf16)
         for o in range(1, chunks):
-            k = lax.rem(c + o, chunks)
-            w2[q, o] = go(
-                copy(
-                    wsend.at[q, k], w2in.at[q, c], "w2", q * chunks + o, "sp", k * GROUPS + m
-                )
-            )
+            w2[q, o].start()
+
+    for q in range(2):
+        add_block(q, me_dp, fresh=True)
+
+    @pl.when(core == 0)
+    def _():
+        add_other_core(0)
+        add_other_core(1)
+        for q in range(2):
+            add_peers(q)
+            scatter(q)
+
+    @pl.when(core != 0)
+    def _():
+        add_peers(0)
+        add_peers(1)
+        for q in range(2):
+            add_other_core(q)
+            scatter(q)
 
     phase("d_hidden")
     for item in w_fwd:
@@ -1014,18 +1085,17 @@
             )
 
     phase("wait_gx")
-    @pl.loop(0, pairs)
-    def _(j):
-        gx_copy(j).wait_recv()
+    all_gx = gx.at[0, : tokens + HALO, :]
+    arrive(copy(all_gx, all_gx, "gx", 0, "sp", partner))
 
     await_edges("gx", gx)
     phase("w3")
     w3 = {}
-    w4 = []
     for q in range(2):
         share = wown[q, c]
+        if chunks > 1:
+            arrive(copy(w2in.at[q, : chunks - 1], w2in.at[q, : chunks - 1], "w2", q, "sp", partner))
         for o in range(1, chunks):
-            arrive(w2[q, o])
             share = share + w2in[q, lax.rem(c - o + chunks, chunks)].astype(f32)
         s3send[q] = share.astype(bf16)
         tall[q, m, c] = s3send[q]
@@ -1033,10 +1103,19 @@
             k = lax.rem(c + o, chunks)
             w3[q, o] = go(
                 copy(
-                    s3send.at[q], tall.at[q, m, c], "w3", q * chunks + o, "sp", k * GROUPS + m
-                )
-            )
-        w4.append(go(copy(s3send.at[q], tall.at[q, m, c], "w4", q * chunks, "sp", partner)))
+                    s3send.at[q],
+                    tall.at[q, m, c],
+                    "w3",
+                    q,
+                    "sp",
+                    k * GROUPS + m,
+                    into=q * (chunks - 1) + o - 1,
+                ),
+                alone=False,
+            )
+        if chunks > 1:
+            together("w3", q, tall.at[q, m, : chunks - 1])
+        go(copy(s3send.at[q], tall.at[q, m, c], "w4", 0, "sp", partner), alone=False)
         phase("dx")
         input_gradient(q)
     phase("w4")
@@ -1044,25 +1123,17 @@
         for o in range(1, chunks):
             arrive(w3[q, o])
             piece = tall.at[q, m, lax.rem(c - o + chunks, chunks)]
-            w4.append(go(copy(piece, piece, "w4", q * chunks + o, "sp", partner)))
+            go(copy(piece, piece, "w4", 0, "sp", partner), alone=False)
     phase("last")
     arrive(ddt_copy)
-    for item in w4:
-        arrive(item)
-
-    @pl.loop(0, pairs)
-    def _(j):
-        gx_copy(j).wait_send()
-
-        @pl.when(jnp.logical_not(last))
-        def _():
-            for q in range(2):
-                chain_copy("right", j, q, rin, rout, GROUPS).wait_send()
-
-        @pl.when(jnp.logical_not(first))
-        def _():
-            for q in range(2):
-                chain_copy("left", j, q, lin, lout, -GROUPS).wait_send()
+    arrive(copy(tall.at[:, p], tall.at[:, p], "w4", 0, "sp", partner))
+    together("w4", 0, tall.at[:, m])
+
+    together("gx", 0, all_gx)
+    for j in range(max(pairs - 2, 0), pairs):
+        for q in range(2):
+            sent.append((chain_copy("right", j, q, rin, rout, GROUPS), jnp.logical_not(last)))
+            sent.append((chain_copy("left", j, q, lin, lout, -GROUPS), jnp.logical_not(first)))
 
     for item, cond in sent:
         if cond is None:
@@ -1138,7 +1209,7 @@
     pairs = gw // LANES
     rows = cw // chunks
     window = tokens * sp
-    _, slots = slot_table(sp, dp, cores, pairs)
+    _, _, send_slots, arrival_slots = slot_tables(sp, dp, cores, pairs)
 
     vmem = pl.BlockSpec(memory_space=pltpu.VMEM)
     hbm = pl.BlockSpec(memory_space=pltpu.HBM)
@@ -1213,6 +1284,7 @@
         ((ch, 2 * STATE), bf16),
         ((GROUPS, tokens, 2 * STATE), bf16),
         ((dp, ch, 2 * STATE), bf16),
+        ((2, STATE, cw), f32),
         ((2, chunks, rows, STATE), bf16),
         ((2, chunks, rows, STATE), f32),
         ((2, chunks, rows, STATE), bf16),
@@ -1230,7 +1302,7 @@
             pltpu.VMEM((2, GROUPS, chunks, rows, STATE), bf16),
         ],
         scratch_shapes=[pltpu.VMEM(shape, kind) for shape, kind in scratch]
-        + [pltpu.SemaphoreType.DMA((slots,)), pltpu.SemaphoreType.DMA((slots,))]
+        + [pltpu.SemaphoreType.DMA((send_slots,)), pltpu.SemaphoreType.DMA((arrival_slots,))]
         + [pltpu.SemaphoreType.DMA((7,))],
         compiler_params=pltpu.CompilerParams(
             collective_id=0, has_side_effects=True, vmem_limit_bytes=60 * 1024 * 1024

time: 75.2 us -> 71.5 us (0.951)
  Pallas kernels: 74.3 us -> 70.6 us
    pallas_call x1, Pallas kernels: 72.7 us -> 69.1 us  [local(): pl.pallas_call(functools.partial(mega_kernel, heads, cores), in_specs=[hb...]
where the time goes in v4:
time: 71.5 us; the launch traced here: 71.3 us
  Pallas kernels  70.6 us (99%)
    pallas_call x1, Pallas kernels, local(): pl.pallas_call(functools.partial(mega_kernel, heads, cores), in_specs=[hb...  69.1 us
    pallas_call x1, Pallas kernels, local(): pl.pallas_call(out_kernel, in_specs=[vmem] * 5, out_specs=[hbm] * 6, scra...  1.54 us

profile of v4, /device:TPU:0, one launch (start us, length us, event | category | flops | bytes accessed | tf_op | source)
XLA Modules:
  0.0 71.3 jit_solution(220265601796767079)
XLA Ops:
  0.6 69.1 %mega.1 = (bf16[128,2048]{1,0:T(8,128)(2,1)S(1)}, bf16[128,2048]{1,0:T(8,128)(2,1)S(1)}, bf16[32,128]{1,0:T(8,128)(2,1)S(1)}, bf16[128,2048]{1,0:T(8,128)(2,1)S(1)}, bf16[2,2,4,128,128]{4,3,2,1,0:T(8,128)(2,1)S(1)}) custom-call(bf16[128,2048]{1,0:T(8,128)(2,1)} %bitcast.18, bf16[512,256]{1,0:T(8,128)(2,1)} %wb_hbm.1, bf16[512,256]{1,0:T(8,128)(2,1)} %wc_hbm.1, ...), custom_call_target="tpu_custom_call" | custom-call | tf_op jit(solution)/shard_map/mega/pallas_call | solution.py:1293
  69.8 1.5 %outputs.1 = (bf16[128,2048]{1,0:T(8,128)(2,1)}, bf16[128,2048]{1,0:T(8,128)(2,1)}, bf16[128,2048]{1,0:T(8,128)(2,1)}, bf16[32,128]{1,0:T(8,128)(2,1)}, f32[512,256]{1,0:T(8,128)}, /*index=5*/f32[512,256]{1,0:T(8,128)}) custom-call(bf16[128,2048]{1,0:T(8,128)(2,1)S(1)} %get-tuple-element.17.dgate, bf16[128,2048]{1,0:T(8,128)(2,1)S(1)} %get-tuple-element.18.dx, ...), custom_call_target="tpu_custom_call" | custom-call | tf_op jit(solution)/shard_map/outputs/pallas_call | solution.py:1329

commit v5 on v4

--- a/solution.py
+++ b/solution.py
@@ -157,15 +157,15 @@
     gates_hbm,
     values_hbm,
     adjoint_hbm,
-    dt_ref,
-    drop_ref,
-    tapx_ref,
-    tapb_ref,
-    tapc_ref,
-    scale_ref,
-    offset_ref,
-    fade_ref,
-    skip_ref,
+    dt_hbm,
+    drop_hbm,
+    tapx_hbm,
+    tapb_hbm,
+    tapc_hbm,
+    scale_hbm,
+    offset_hbm,
+    fade_hbm,
+    skip_hbm,
     dgate_ref,
     dx_ref,
     ddt_ref,
@@ -178,6 +178,15 @@
     gates_ref,
     values_ref,
     adjoint_ref,
+    dt_ref,
+    drop_ref,
+    tapx_ref,
+    tapb_ref,
+    tapc_ref,
+    scale_ref,
+    offset_ref,
+    fade_ref,
+    skip_ref,
     wball,
     wcall,
     cols,
@@ -338,10 +347,19 @@
             (gates_hbm, gates_ref),
             (adjoint_hbm, adjoint_ref),
             (la_hbm, la_ref),
+            (dt_hbm, dt_ref),
+            (drop_hbm, drop_ref),
+            (tapx_hbm, tapx_ref),
+            (tapb_hbm, tapb_ref),
+            (tapc_hbm, tapc_ref),
+            (scale_hbm, scale_ref),
+            (offset_hbm, offset_ref),
+            (fade_hbm, fade_ref),
+            (skip_hbm, skip_ref),
         )
     ):
         loads[at] = pltpu.make_async_copy(source, target, ls.at[at])
-    for at in (6, 2, 0, 1, 3, 4, 5):
+    for at in (6, 2, 0, 1, *range(7, 16), 3, 4, 5):
         loads[at].start()
     greet(("dp", "sp"))
     loads[6].wait()
@@ -374,6 +392,8 @@
             go(copy(wb_ref, wball.at[me_dp], "w_core", 0, "dp", other_core)),
             go(copy(wc_ref, wcall.at[me_dp], "w_core", 1, "dp", other_core)),
         ]
+    for at in range(7, 16):
+        loads[at].wait()
     dt_copy = go(
         copy(
             dt_ref.at[pl.ds(pl.multiple_of(p * gh, gh), gh), :],
@@ -441,9 +461,14 @@
     head_row = lax.broadcasted_iota(jnp.int32, (rows_h, LANES), 0)
     offsets = jnp.zeros((rows_h, LANES), f32)
     fades = jnp.zeros((rows_h, LANES), f32)
+    head_lane = lax.broadcasted_iota(jnp.int32, (1, heads), 1)
+
+    def pick(ref, h):
+        return jnp.sum(jnp.where(head_lane == h, ref[...], 0.0), axis=1, keepdims=True)
+
     for h in range(heads):
-        offsets = jnp.where(head_row == h, offset_ref[h], offsets)
-        fades = jnp.where(head_row == h, fade_ref[h], fades)
+        offsets = jnp.where(head_row == h, pick(offset_ref, h), offsets)
+        fades = jnp.where(head_row == h, pick(fade_ref, h), fades)
     dropsend[...] = jnp.zeros_like(dropsend)
     for k in range(chunks):
         dropsend[k, :heads, :ch] = drop_ref[:, k * ch : (k + 1) * ch]
@@ -477,7 +502,7 @@
     tap_lane = lax.broadcasted_iota(jnp.int32, (1, xw), 1) // HEAD_DIM
     skips = jnp.zeros((1, xw), f32)
     for h in range(heads):
-        skips = jnp.where(tap_lane == h, skip_ref[h], skips)
+        skips = jnp.where(tap_lane == h, pick(skip_ref, h), skips)
     tapsend[...] = jnp.zeros_like(tapsend)
     tapsend[:CONV_K, :xc] = tapx_ref[...]
     tapsend[CONV_K : CONV_K + 1, :] = skips
@@ -588,6 +613,29 @@
         total_b, total_c = (one, two) if k == 0 else (total_b + one, total_c + two)
     psum[:, :latent] = total_b
     psum[:, latent:] = total_c
+    phase("project")
+    bc_copies = []
+    for t in range(PIECES):
+        total = psum[parts[t], :]
+        for o in range(1, ny):
+            arrive(p_y[o, t])
+            total = total + pin[lax.rem(y - o + ny, ny), parts[t], :].astype(f32)
+        total = total.astype(bf16)
+        for g in range(GROUPS):
+            at = slice(g * STATE, (g + 1) * STATE)
+            bcsend[g, parts[t], :STATE] = total[:, at]
+            at = slice(latent + g * STATE, latent + (g + 1) * STATE)
+            bcsend[g, parts[t], STATE:] = total[:, at]
+        into = pl.ds(pl.multiple_of(HALO + m * tokens + t * part_rows, HALO), part_rows)
+        bc_copies.append(
+            go(copy(bcsend.at[p, parts[t], :], bcin.at[into, :], "bc", t, "sp", partner))
+        )
+    send_halo("bc", lambda g, r: bcsend.at[g, r, :], bcin)
+    bcin[mine, :] = bcsend[m]
+    for item in dy_copies[early:]:
+        go(item, alone=False)
+    together("dy", 0, dysend)
+
     phase("levels")
     arrive(dt_copy)
     if nsrc > 1:
@@ -625,29 +673,6 @@
         tdec[j] = jnp.broadcast_to(jnp.exp2(-end), (8, LANES))
         dts_ref[j] = jnp.where(low_lane, dtcol[:, 2 * j : 2 * j + 1], dtcol[:, 2 * j + 1 : 2 * j + 2])
 
-    phase("project")
-    bc_copies = []
-    for t in range(PIECES):
-        total = psum[parts[t], :]
-        for o in range(1, ny):
-            arrive(p_y[o, t])
-            total = total + pin[lax.rem(y - o + ny, ny), parts[t], :].astype(f32)
-        total = total.astype(bf16)
-        for g in range(GROUPS):
-            at = slice(g * STATE, (g + 1) * STATE)
-            bcsend[g, parts[t], :STATE] = total[:, at]
-            at = slice(latent + g * STATE, latent + (g + 1) * STATE)
-            bcsend[g, parts[t], STATE:] = total[:, at]
-        into = pl.ds(pl.multiple_of(HALO + m * tokens + t * part_rows, HALO), part_rows)
-        bc_copies.append(
-            go(copy(bcsend.at[p, parts[t], :], bcin.at[into, :], "bc", t, "sp", partner))
-        )
-    send_halo("bc", lambda g, r: bcsend.at[g, r, :], bcin)
-    bcin[mine, :] = bcsend[m]
-    for item in dy_copies[early:]:
-        go(item, alone=False)
-    together("dy", 0, dysend)
-
     phase("wait_x")
     arrive(copy(all_taps, all_taps, "tap", 0, "sp", partner))
     if xc % LANES == 0:
@@ -842,19 +867,19 @@
             sl_ref[tick, 0] = mm(kt[...], vef_ref[tick])
             sl_ref[tick, 1] = mm(rt[...], dyef_ref[tick])
 
+        jl = tick - SKEW * (chunks - 1 - c)
+
+        @pl.when(jnp.logical_and(jl >= 0, jl < pairs))
+        def _():
+            with jax.named_scope("chain_l"):
+                chain("left", jl, lin, sl_ref, lout, last, first, -GROUPS)
+
         jr = tick - SKEW * c
 
         @pl.when(jnp.logical_and(jr >= 0, jr < pairs))
         def _():
             with jax.named_scope("chain_r"):
                 chain("right", jr, rin, sr_ref, rout, first, last, GROUPS)
-
-        jl = tick - SKEW * (chunks - 1 - c)
-
-        @pl.when(jnp.logical_and(jl >= 0, jl < pairs))
-        def _():
-            with jax.named_scope("chain_l"):
-                chain("left", jl, lin, sl_ref, lout, last, first, -GROUPS)
 
         @pl.when(tick < pairs)
         def _():
@@ -940,27 +965,6 @@
     gx_copy(pairs - 1).start()
     send_edges("gx", dpx, gx)
 
-    phase("ddt")
-    w_fwd = []
-    for o in range(1, ny):
-        src = lax.rem(y - o + ny, ny) * cores + core
-        for q in range(2):
-            arrive(w_y[o - 1][q])
-            if cores > 1:
-                full = (wball, wcall)[q].at[src]
-                w_fwd.append(go(copy(full, full, "w_fwd", 2 * o - 2 + q, "dp", other_core)))
-
-    fill = jnp.zeros((LANES - gh, ch), f32)
-    down = jnp.concatenate([colrow[...], fill], axis=0).T
-    drate = jnp.dot(upper, dlev[...] - down, precision=highest, preferred_element_type=f32)
-    drate = (drate - cross[0:1, :]).T[:gh]
-    ddt = ((drate * twice(faderow[...]) + sdt[...].T[:gh]) * sigrow[...]).astype(bf16)
-    for g in range(GROUPS):
-        ddtsend[g] = ddt[:, g * tokens : (g + 1) * tokens]
-    group_rows = pl.ds(pl.multiple_of(m * gh, gh), gh)
-    ddt_copy = go(copy(ddtsend.at[p], ddt_ref.at[group_rows, :], "ddt", 0, "sp", partner))
-    ddt_ref[group_rows, :] = ddtsend[m]
-
     phase("wait_db")
     await_halo("db", dbin)
     phase("conv_g")
@@ -996,6 +1000,27 @@
     hid_copy = go(copy(gsend.at[theirs, :], ghid.at[m], "gx_g", 0, "sp", partner))
     ghid[m] = gsend[mine0, :]
     gall[me_dp] = gsend[...]
+    phase("ddt")
+    w_fwd = []
+    for o in range(1, ny):
+        src = lax.rem(y - o + ny, ny) * cores + core
+        for q in range(2):
+            arrive(w_y[o - 1][q])
+            if cores > 1:
+                full = (wball, wcall)[q].at[src]
+                w_fwd.append(go(copy(full, full, "w_fwd", 2 * o - 2 + q, "dp", other_core)))
+
+    fill = jnp.zeros((LANES - gh, ch), f32)
+    down = jnp.concatenate([colrow[...], fill], axis=0).T
+    drate = jnp.dot(upper, dlev[...] - down, precision=highest, preferred_element_type=f32)
+    drate = (drate - cross[0:1, :]).T[:gh]
+    ddt = ((drate * twice(faderow[...]) + sdt[...].T[:gh]) * sigrow[...]).astype(bf16)
+    for g in range(GROUPS):
+        ddtsend[g] = ddt[:, g * tokens : (g + 1) * tokens]
+    group_rows = pl.ds(pl.multiple_of(m * gh, gh), gh)
+    ddt_copy = go(copy(ddtsend.at[p], ddt_ref.at[group_rows, :], "ddt", 0, "sp", partner))
+    ddt_ref[group_rows, :] = ddtsend[m]
+
     phase("wait_g")
     arrive(cols_copy)
     sources = {o: lax.rem(y - o + ny, ny) * cores + core for o in range(1, ny)}
@@ -1213,7 +1238,6 @@
 
     vmem = pl.BlockSpec(memory_space=pltpu.VMEM)
     hbm = pl.BlockSpec(memory_space=pltpu.HBM)
-    smem = pl.BlockSpec(memory_space=pltpu.SMEM)
     scratch = [
         ((tokens, width_in), bf16),
         ((cw, latent), bf16),
@@ -1222,6 +1246,15 @@
         ((tokens, inner), bf16),
         ((tokens, inner), bf16),
         ((tokens, inner), bf16),
+        ((HEADS, tokens), bf16),
+        ((heads, window), f32),
+        ((CONV_K, xc), f32),
+        ((CONV_K, latent), f32),
+        ((CONV_K, latent), f32),
+        ((1, inner), f32),
+        ((1, heads), f32),
+        ((1, heads), f32),
+        ((1, heads), f32),
         ((dp, cw, latent), bf16),
         ((dp, cw, latent), bf16),
         ((GROUPS, dp, tokens, cw), bf16),
@@ -1292,7 +1325,7 @@
     ]
     dgate, dx, ddt, dh, tall = pl.pallas_call(
         functools.partial(mega_kernel, heads, cores),
-        in_specs=[hbm] * 7 + [vmem] * 6 + [smem] * 3,
+        in_specs=[hbm] * 16,
         out_specs=[vmem] * 5,
         out_shape=[
             pltpu.VMEM((tokens, inner), bf16),
@@ -1303,7 +1336,7 @@
         ],
         scratch_shapes=[pltpu.VMEM(shape, kind) for shape, kind in scratch]
         + [pltpu.SemaphoreType.DMA((send_slots,)), pltpu.SemaphoreType.DMA((arrival_slots,))]
-        + [pltpu.SemaphoreType.DMA((7,))],
+        + [pltpu.SemaphoreType.DMA((16,))],
         compiler_params=pltpu.CompilerParams(
             collective_id=0, has_side_effects=True, vmem_limit_bytes=60 * 1024 * 1024
         ),
@@ -1322,9 +1355,9 @@
         writer_filter_coefs,
         reader_filter_coefs,
         rescale_factor.reshape(1, inner),
-        delta_offset,
-        fading_exponents,
-        direct_factor,
+        delta_offset.reshape(1, heads),
+        fading_exponents.reshape(1, heads),
+        direct_factor.reshape(1, heads),
     )
     d_gate, d_x, d_hidden, d_dt, d_w_b, d_w_c = pl.pallas_call(
         out_kernel,

time: 71.5 us -> 69.3 us (0.969)
  Pallas kernels: 70.6 us -> 68.5 us
    pallas_call x1, Pallas kernels: 69.1 us -> 66.9 us  [local(): pl.pallas_call(functools.partial(mega_kernel, heads, cores), in_specs=[hb...]
where the time goes in v5:
time: 69.3 us; the launch traced here: 69.1 us
  Pallas kernels  68.5 us (99%)
    pallas_call x1, Pallas kernels, local(): pl.pallas_call(functools.partial(mega_kernel, heads, cores), in_specs=[hb...  66.9 us
    pallas_call x1, Pallas kernels, local(): pl.pallas_call(out_kernel, in_specs=[vmem] * 5, out_specs=[hbm] * 6, scra...  1.54 us

profile of v5, /device:TPU:0, one launch (start us, length us, event | category | flops | bytes accessed | tf_op | source)
XLA Modules:
  0.0 69.1 jit_solution(11731755426674579415)
XLA Ops:
  0.6 66.9 %mega.1 = (bf16[128,2048]{1,0:T(8,128)(2,1)S(1)}, bf16[128,2048]{1,0:T(8,128)(2,1)S(1)}, bf16[32,128]{1,0:T(8,128)(2,1)S(1)}, bf16[128,2048]{1,0:T(8,128)(2,1)S(1)}, bf16[2,2,4,128,128]{4,3,2,1,0:T(8,128)(2,1)S(1)}) custom-call(bf16[128,2048]{1,0:T(8,128)(2,1)} %bitcast.21, bf16[512,256]{1,0:T(8,128)(2,1)} %wb_hbm.1, bf16[512,256]{1,0:T(8,128)(2,1)} %wc_hbm.1, ...), custom_call_target="tpu_custom_call" | custom-call | tf_op jit(solution)/shard_map/mega/pallas_call | solution.py:1326
  67.6 1.5 %outputs.1 = (bf16[128,2048]{1,0:T(8,128)(2,1)}, bf16[128,2048]{1,0:T(8,128)(2,1)}, bf16[128,2048]{1,0:T(8,128)(2,1)}, bf16[32,128]{1,0:T(8,128)(2,1)}, f32[512,256]{1,0:T(8,128)}, /*index=5*/f32[512,256]{1,0:T(8,128)}) custom-call(bf16[128,2048]{1,0:T(8,128)(2,1)S(1)} %get-tuple-element.17.dgate, bf16[128,2048]{1,0:T(8,128)(2,1)S(1)} %get-tuple-element.18.dx, ...), custom_call_target="tpu_custom_call" | custom-call | tf_op jit(solution)/shard_map/outputs/pallas_call | solution.py:1362

commit v6 on v5

--- a/solution.py
+++ b/solution.py
@@ -103,7 +103,6 @@
 def slot_tables(sp, dp, cores, pairs):
     others = dp // cores - 1
     chunks = sp // GROUPS
-    away = max(chunks - 1, 1)
     counts = (
         ("w_y", 2 * others, 2 * others),
         ("w_core", 2, 2),
@@ -135,7 +134,7 @@
         ("g_core", 2, 2),
         ("g_fwd", 2 * others, 2 * others),
         ("w2", 2, 2),
-        ("w3", 2, 2 * away),
+        ("w3", 2, 2 * chunks),
         ("w4", 1, 1),
     )
     sends, arrivals = {}, {}
@@ -580,15 +579,6 @@
                     there * cores + core,
                 )
             )
-    w_y = []
-    for o in range(1, ny):
-        peer = lax.rem(y + o, ny) * cores + core
-        w_y.append(
-            (
-                go(copy(wb_ref, wball.at[me_dp], "w_y", 2 * o - 2, "dp", peer)),
-                go(copy(wc_ref, wcall.at[me_dp], "w_y", 2 * o - 1, "dp", peer)),
-            )
-        )
     for o in range(1, ny):
         there = lax.rem(y - o + ny, ny)
         block = there * cores + core
@@ -632,9 +622,6 @@
         )
     send_halo("bc", lambda g, r: bcsend.at[g, r, :], bcin)
     bcin[mine, :] = bcsend[m]
-    for item in dy_copies[early:]:
-        go(item, alone=False)
-    together("dy", 0, dysend)
 
     phase("levels")
     arrive(dt_copy)
@@ -702,6 +689,9 @@
         veb_ref[j] = (v * eb_ref[j]).astype(bf16)
 
     phase("wait_bc")
+    for item in dy_copies[early:]:
+        go(item, alone=False)
+    together("dy", 0, dysend)
     for item in bc_copies:
         arrive(item)
     await_halo("bc", bcin)
@@ -845,6 +835,15 @@
 
     for item in la_copies:
         arrive(item)
+    w_y = []
+    for o in range(1, ny):
+        peer = lax.rem(y + o, ny) * cores + core
+        w_y.append(
+            (
+                go(copy(wb_ref, wball.at[me_dp], "w_y", 2 * o - 2, "dp", peer)),
+                go(copy(wc_ref, wcall.at[me_dp], "w_y", 2 * o - 1, "dp", peer)),
+            )
+        )
     cols_copy = go(copy(cols.at[m], cols.at[m], "cols", 0, "sp", partner))
     phase("ticks")
     @pl.loop(0, pairs + delay)
@@ -1026,7 +1025,6 @@
     sources = {o: lax.rem(y - o + ny, ny) * cores + core for o in range(1, ny)}
     relayed = {o: lax.rem(y - o + ny, ny) * cores + cores - 1 - core for o in range(1, ny)}
     g_fwd = {}
-    w2 = {}
     for q in range(2):
         for o in range(1, ny):
             if cores > 1:
@@ -1035,13 +1033,16 @@
                     block, block, "g_fwd", 2 * (o - 1) + q, "dp", other_core
                 )
                 sent.append((g_fwd[o, q], None))
-        for o in range(1, chunks):
-            k = lax.rem(c + o, chunks)
-            w2[q, o] = copy(
-                wsend.at[q, k], w2in.at[q, c], "w2", q, "sp", k * GROUPS + m
-            )
         if chunks > 1:
             together("w2", q, w2in.at[q, : chunks - 1])
+
+    def by_distance(distances, act):
+        for d in distances:
+            for k in (c + d, c - d):
+
+                @pl.when(jnp.logical_and(k >= 0, k < chunks))
+                def _():
+                    act(k)
 
     def add_block(q, i, fresh=False):
         total = None
@@ -1069,8 +1070,11 @@
         total = wtot[q].T.reshape(chunks, rows, STATE)
         wown[q] = total
         wsend[q] = total.astype(bf16)
-        for o in range(1, chunks):
-            w2[q, o].start()
+
+        def send(k):
+            copy(wsend.at[q, k], w2in.at[q, c], "w2", q, "sp", k * GROUPS + m).start()
+
+        by_distance(reversed(range(1, chunks)), send)
 
     for q in range(2):
         add_block(q, me_dp, fresh=True)
@@ -1115,7 +1119,6 @@
 
     await_edges("gx", gx)
     phase("w3")
-    w3 = {}
     for q in range(2):
         share = wown[q, c]
         if chunks > 1:
@@ -1124,20 +1127,19 @@
             share = share + w2in[q, lax.rem(c - o + chunks, chunks)].astype(f32)
         s3send[q] = share.astype(bf16)
         tall[q, m, c] = s3send[q]
-        for o in range(1, chunks):
-            k = lax.rem(c + o, chunks)
-            w3[q, o] = go(
-                copy(
-                    s3send.at[q],
-                    tall.at[q, m, c],
-                    "w3",
-                    q,
-                    "sp",
-                    k * GROUPS + m,
-                    into=q * (chunks - 1) + o - 1,
-                ),
-                alone=False,
-            )
+
+        def share_out(k):
+            copy(
+                s3send.at[q],
+                tall.at[q, m, c],
+                "w3",
+                q,
+                "sp",
+                k * GROUPS + m,
+                into=q * chunks + c,
+            ).start()
+
+        by_distance(reversed(range(1, chunks)), share_out)
         if chunks > 1:
             together("w3", q, tall.at[q, m, : chunks - 1])
         go(copy(s3send.at[q], tall.at[q, m, c], "w4", 0, "sp", partner), alone=False)
@@ -1145,10 +1147,13 @@
         input_gradient(q)
     phase("w4")
     for q in range(2):
-        for o in range(1, chunks):
-            arrive(w3[q, o])
-            piece = tall.at[q, m, lax.rem(c - o + chunks, chunks)]
-            go(copy(piece, piece, "w4", 0, "sp", partner), alone=False)
+
+        def pass_on(k):
+            piece = tall.at[q, m, k]
+            copy(piece, piece, "w3", q, "sp", partner, into=q * chunks + k).wait_recv()
+            copy(piece, piece, "w4", 0, "sp", partner).start()
+
+        by_distance(range(1, chunks), pass_on)
     phase("last")
     arrive(ddt_copy)
     arrive(copy(tall.at[:, p], tall.at[:, p], "w4", 0, "sp", partner))

time: 69.3 us -> 68.7 us (level)
  no operation moved by 1% of the time
where the time goes in v6:
time: 68.7 us; the launch traced here: 68.5 us
  Pallas kernels  67.9 us (99%)
    pallas_call x1, Pallas kernels, local(): pl.pallas_call(functools.partial(mega_kernel, heads, cores), in_specs=[hb...  66.3 us
    pallas_call x1, Pallas kernels, local(): pl.pallas_call(out_kernel, in_specs=[vmem] * 5, out_specs=[hbm] * 6, scra...  1.54 us

profile of v6, /device:TPU:0, one launch (start us, length us, event | category | flops | bytes accessed | tf_op | source)
XLA Modules:
  0.0 68.5 jit_solution(5818239043952460178)
XLA Ops:
  0.6 66.3 %mega.1 = (bf16[128,2048]{1,0:T(8,128)(2,1)S(1)}, bf16[128,2048]{1,0:T(8,128)(2,1)S(1)}, bf16[32,128]{1,0:T(8,128)(2,1)S(1)}, bf16[128,2048]{1,0:T(8,128)(2,1)S(1)}, bf16[2,2,4,128,128]{4,3,2,1,0:T(8,128)(2,1)S(1)}) custom-call(bf16[128,2048]{1,0:T(8,128)(2,1)} %bitcast.21, bf16[512,256]{1,0:T(8,128)(2,1)} %wb_hbm.1, bf16[512,256]{1,0:T(8,128)(2,1)} %wc_hbm.1, ...), custom_call_target="tpu_custom_call" | custom-call | tf_op jit(solution)/shard_map/mega/pallas_call | solution.py:1331
  67.0 1.5 %outputs.1 = (bf16[128,2048]{1,0:T(8,128)(2,1)}, bf16[128,2048]{1,0:T(8,128)(2,1)}, bf16[128,2048]{1,0:T(8,128)(2,1)}, bf16[32,128]{1,0:T(8,128)(2,1)}, f32[512,256]{1,0:T(8,128)}, /*index=5*/f32[512,256]{1,0:T(8,128)}) custom-call(bf16[128,2048]{1,0:T(8,128)(2,1)S(1)} %get-tuple-element.17.dgate, bf16[128,2048]{1,0:T(8,128)(2,1)S(1)} %get-tuple-element.18.dx, ...), custom_call_target="tpu_custom_call" | custom-call | tf_op jit(solution)/shard_map/outputs/pallas_call | solution.py:1367
